TPU v7x, 32 devices: a whole 2x2x4 slice. The times are simulated.
32 devices in a mesh: gr: 2 (over x), sp: 8 (over z, y), tp: 2 (over core).
Axes of the slice: x: 2, y: 2, z: 4, core: 2. Of those that a mesh axis runs over, the one named last changes fastest.
Arguments:
- tokens: bfloat16 [8, 1024, 4096], P('gr', 'sp'), parts along dimension 0, may hold values from -6 to 6
- key_weight: bfloat16 [4096, 2048], P('sp', 'tp'), may hold values from -0.09375 to 0.09375
- value_weight: bfloat16 [4096, 2048], P('sp', 'tp'), may hold values from -0.09375 to 0.09375
- log_decay: float32 [32, 8, 1024], P('tp', 'gr', 'sp'), parts along dimension 1, may hold values from -1 to 0, as said below
- new_query: bfloat16 [8, 2048], P('gr', 'tp'), parts along dimension 0, may hold values from -6 to 6
- new_key: bfloat16 [8, 2048], P('gr', 'tp'), parts along dimension 0, may hold values from -24 to 24
- new_value: bfloat16 [8, 2048], P('gr', 'tp'), parts along dimension 0, may hold values from -6 to 6
- step_decay: float32 [32, 8], P('tp', 'gr'), parts along dimension 1, may hold values from -1.5 to -0.05
- norm_gain: float32 [2048], P('tp'), may hold values from 0.1 to 1.9
Outputs:
- state_cache: float32 [512, 32, 64], P('gr', 'tp'), parts along dimension 0
- first_read: bfloat16 [8, 2048], P('gr', 'tp'), parts along dimension 0
There are 2 independent parts, one for each index of `gr`. A program takes and returns all parts, laid end to end along the dimension named above; an argument that names none is the same for every part. Nothing has to cross between parts.
Inputs may be any that keep to these rules, and one draw needn't show every extreme that they name: `log_decay`: every entry is at most zero.
All inputs are finite; a program needn't handle non-finite values.
Results may differ from a plain program's by a relative error of at most 0.0053.
Values may be sent and summed in bfloat16 or wider, within the bound.
A program may use at most 64 MiB of HBM per device.

v0:
```python
import functools

import jax
import jax.numpy as jnp
import numpy as np
from jax import lax
from jax.experimental import pallas as pl
from jax.experimental.pallas import tpu as pltpu
from jax.sharding import PartitionSpec as P

HEAD_DIM = 64
SUB = 4
MESH = pl.DeviceIdType.MESH
F32 = jnp.float32
HIGH = lax.Precision.HIGHEST


def kernel(
    sizes,
    tok, kw, vw, ld, cos_tab, sin_tab, nq, nk, nv, sd, gain,
    out, read,
    toks, w, kv, acc, lds, tots, part, got, full, cos_ref, sin_ref, ends, qx, outer, decay,
    l_sem, tok_s, tok_r, core_s, core_r, yw_s, yw_r, up_s, dn_s, z_r, x_s, x_r,
    ld_s, ld_r, tot_s, tot_r, rs_s, rs_r, ag_s, ag_r, yg_s, yg_r,
):
    n_sp, seqs, span, heads = sizes
    n_a = n_sp // 2
    g, sp, tp = lax.axis_index("gr"), lax.axis_index("sp"), lax.axis_index("tp")
    a, b = sp // 2, sp % 2
    ob = 1 - b
    core = tp % 2
    mate = tp + 1 - 2 * core
    rows, width = tok.shape
    depth = kw.shape[0]
    cols = kw.shape[1] // 2
    piece = depth // SUB
    half = rows // 2
    hs = heads * seqs
    y_peer = (g, a * 2 + ob, tp)
    x_peer = (1 - g, sp, tp)
    core_peer = (g, sp, mate)

    def mine(col_half):
        return pl.ds(pl.multiple_of(col_half * cols, 128), cols)

    def shard_rows(s, q=None):
        if q is None:
            return pl.ds(pl.multiple_of(s * depth, depth), depth)
        return pl.ds(pl.multiple_of(s * depth + q * piece, piece), piece)

    local = [
        pltpu.make_async_copy(kw.at[:, mine(b)], w.at[0, shard_rows(sp)], l_sem.at[0]),
        pltpu.make_async_copy(vw.at[:, mine(b)], w.at[1, shard_rows(sp)], l_sem.at[1]),
        pltpu.make_async_copy(tok, toks.at[b], l_sem.at[2]),
        pltpu.make_async_copy(ld, lds.at[b], l_sem.at[3]),
        pltpu.make_async_copy(cos_tab.at[pl.ds(pl.multiple_of(a * 2 * span, 8), 2 * span)], cos_ref, l_sem.at[4]),
        pltpu.make_async_copy(sin_tab.at[pl.ds(pl.multiple_of(a * 2 * span, 8), 2 * span)], sin_ref, l_sem.at[5]),
        pltpu.make_async_copy(cos_tab.at[pl.ds(n_sp * span, 8)], ends.at[0], l_sem.at[6]),
        pltpu.make_async_copy(sin_tab.at[pl.ds(n_sp * span, 8)], ends.at[1], l_sem.at[7]),
    ]
    for c in local:
        c.start()

    barrier = pltpu.get_barrier_semaphore()

    @pl.loop(1, n_sp)
    def _(k):
        pl.semaphore_signal(barrier, inc=1, device_id=(g, lax.rem(sp + k, n_sp), tp), device_id_type=MESH)

    pl.semaphore_signal(barrier, inc=1, device_id=x_peer, device_id_type=MESH)
    pl.semaphore_signal(barrier, inc=1, device_id=core_peer, device_id_type=MESH)
    pl.semaphore_wait(barrier, n_sp + 1)

    def remote(src, dst, s, r, dev):
        return pltpu.make_async_remote_copy(
            src_ref=src, dst_ref=dst, send_sem=s, recv_sem=r, device_id=dev, device_id_type=MESH
        )

    def yw(m, q):
        src = (kw, vw)[m].at[pl.ds(q * piece, piece), mine(ob)]
        return remote(src, w.at[m, shard_rows(sp, q)], yw_s.at[m, q], yw_r.at[m, q], y_peer)

    half_rows = pl.ds(pl.multiple_of(core * half, half), half)
    ytok = remote(tok.at[half_rows], toks.at[b, half_rows], tok_s, tok_r, y_peer)
    yld = remote(ld, lds.at[b], ld_s, ld_r, y_peer)

    for m in range(2):
        @pl.when(g == m)
        def _():
            for q in range(SUB):
                yw(m, q).start()
            yld.start()
            ytok.start()
            for q in range(SUB):
                yw(1 - m, q).start()

    local[0].wait()
    local[1].wait()

    def zsend(s, q, up):
        ref = w.at[g, shard_rows(s, q)]
        sem = (up_s if up else dn_s).at[s, q]
        return remote(ref, ref, sem, z_r.at[s, q], (g, sp + (2 if up else -2), tp))

    def xsend(s, q):
        ref = w.at[g, shard_rows(s, q)]
        return remote(ref, ref, x_s.at[s, q], x_r.at[s, q], x_peer)

    def xrecv(s, q):
        ref = w.at[1 - g, shard_rows(s, q)]
        return remote(ref, ref, x_s.at[s, q], x_r.at[s, q], x_peer)

    def launch(s, q):
        @pl.when(a < n_a - 1)
        def _():
            zsend(s, q, True).start()

        @pl.when(a > 0)
        def _():
            zsend(s, q, False).start()

    for q in range(SUB):
        launch(sp, q)

    def tsend(k):
        return remote(tots.at[sp], tots.at[sp], tot_s.at[k], tot_r.at[k], (g, lax.rem(sp + k, n_sp), tp))

    for c in local[2:]:
        c.wait()
    tots[sp] = jnp.zeros(tots.shape[1:], F32)
    tots[sp, :, 0:hs] = lax.dot_general(
        jnp.ones((8, span), F32), lds[b], (((1,), (1,)), ((), ())), precision=HIGH, preferred_element_type=F32
    )

    lanes = lax.broadcasted_iota(jnp.int32, (HEAD_DIM, 128), 1)
    subs = lax.broadcasted_iota(jnp.int32, (HEAD_DIM, 128), 0)
    diagonal = lanes % HEAD_DIM == subs
    same_head = jnp.where(
        lax.broadcasted_iota(jnp.int32, (128, 128), 0) // HEAD_DIM
        == lax.broadcasted_iota(jnp.int32, (128, 128), 1) // HEAD_DIM, 1.0, 0.0
    ).astype(F32)

    def exact(x, y):
        return jnp.dot(x, y, precision=HIGH, preferred_element_type=F32)

    def at_end(u):
        low = lax.broadcasted_iota(jnp.int32, u.shape, 1) % HEAD_DIM < HEAD_DIM // 2
        turned = jnp.where(low, pltpu.roll(u, 128 - 32, 1), pltpu.roll(u, 32, 1))
        return u * ends[0, 0:1, :] + turned * ends[1, 0:1, :]

    head_lane = lax.broadcasted_iota(jnp.int32, (heads, 2 * cols), 1) // HEAD_DIM
    head_row = lax.broadcasted_iota(jnp.int32, (heads, 2 * cols), 0)
    spread_heads = jnp.where(head_lane == head_row, 1.0, 0.0).astype(F32)
    decay[...] = jnp.exp(exact(sd[...], spread_heads))

    def new_token(c0):
        chunk = pl.ds(c0, 128)
        query = at_end(nq[:, chunk].astype(F32)) * HEAD_DIM ** 0.5
        key_new = at_end(nk[:, chunk].astype(F32))
        value_new = nv[:, chunk].astype(F32)
        for s in range(seqs):
            at = pl.ds(s * HEAD_DIM, HEAD_DIM)
            qx[at, chunk] = exact(jnp.where(diagonal, query[s:s + 1], 0.0), same_head)
            column = exact(jnp.where(diagonal, key_new[s:s + 1], 0.0), same_head)
            outer[at, chunk] = column * value_new[s:s + 1]

    def zstep(d, bb, q):
        below = (a - d) * 2 + (b if bb == 0 else ob)
        above = (a + d) * 2 + (b if bb == 0 else ob)

        @pl.when(a - d >= 0)
        def _():
            zsend(below, q, True).wait_recv()

            @pl.when(a < n_a - 1)
            def _():
                zsend(below, q, True).start()

            xsend(below, q).start()

        @pl.when(a + d < n_a)
        def _():
            zsend(above, q, False).wait_recv()

            @pl.when(a > 0)
            def _():
                zsend(above, q, False).start()

            xsend(above, q).start()

    chunks = list(range(0, 2 * cols, 128))
    for q in range(SUB):
        for m in range(2):
            @pl.when(g == m)
            def _():
                yw(m, q).wait_recv()
        launch(a * 2 + ob, q)
        zstep(1, 0, q)
        for c0 in chunks[q::SUB]:
            new_token(c0)

    @pl.loop(1, n_sp)
    def _(k):
        tsend(k).start()

    tile = min(256, rows)

    def own_product(m, s, fresh=False):
        depth_at = shard_rows(s)

        @pl.loop(0, rows // tile)
        def _(r):
            at = pl.ds(pl.multiple_of(r * tile, tile), tile)
            new = jnp.dot(toks[b, at, depth_at], w[m, depth_at, :], preferred_element_type=F32)
            acc[m, at, :] = new if fresh else acc[m, at, :] + new

    own_product(0, sp, True)
    own_product(1, sp, True)
    own_product(g, a * 2 + ob)

    def take(d, bb, mats):
        side = b if bb == 0 else ob
        for inside, s in ((a - d >= 0, (a - d) * 2 + side), (a + d < n_a, (a + d) * 2 + side)):
            @pl.when(inside)
            def _():
                if 0 in mats:
                    own_product(g, s)
                if 1 in mats:
                    for q in range(SUB):
                        xrecv(s, q).wait_recv()
                    own_product(1 - g, s)

    for q in range(SUB):
        zstep(1, 1, q)

    @pl.loop(2, n_a)
    def _(d):
        for bb in range(2):
            for q in range(SUB):
                zstep(d, bb, q)
            take(d - 1, bb, (0, 1))

    ytok_in = remote(toks.at[ob, half_rows], toks.at[ob, half_rows], tok_s, tok_r, y_peer)
    ctok = remote(toks.at[ob, half_rows], toks.at[ob, half_rows], core_s, core_r, core_peer)
    ytok_in.wait_recv()
    ctok.start()
    yld.wait_recv()

    @pl.loop(1, n_sp)
    def _(k):
        tsend(k).wait_recv()

    pos_t = lax.broadcasted_iota(jnp.int32, (span, span), 0)
    pos_u = lax.broadcasted_iota(jnp.int32, (span, span), 1)
    later_mask = jnp.where(pos_u > pos_t, 1.0, 0.0).astype(F32)
    suffix = []
    for tb in range(2):
        inside = lax.dot_general(
            later_mask, lds[tb], (((1,), (1,)), ((), ())), precision=HIGH, preferred_element_type=F32
        )
        index = a * 2 + tb

        def add(k, total):
            return total + jnp.where(k > index, tots[k], 0.0)

        after = lax.fori_loop(0, n_sp, add, jnp.zeros(tots.shape[1:], F32))
        suffix.append(inside + after[0:1, :hs])
    row_hs = lax.broadcasted_iota(jnp.int32, (hs, cols), 0)
    lane_head = lax.broadcasted_iota(jnp.int32, (hs, cols), 1) // HEAD_DIM + b * (heads // 2)

    def partner_product(m):
        @pl.loop(0, rows // tile)
        def _(r):
            at = pl.ds(pl.multiple_of(r * tile, tile), tile)
            new = jnp.dot(toks[ob, at, :], w[m], preferred_element_type=F32)
            kv[m, ob, at, :] = new.astype(jnp.bfloat16)
            kv[m, b, at, :] = acc[m, at, :].astype(jnp.bfloat16)

    for bb in range(2):
        take(n_a - 1, bb, (0,))
    ctok.wait_recv()
    partner_product(g)
    for q in range(SUB):
        for m in range(2):
            @pl.when(g == m)
            def _():
                yw(1 - m, q).wait_recv()
    own_product(1 - g, a * 2 + ob)
    for bb in range(2):
        take(n_a - 1, bb, (1,))
    partner_product(1 - g)

    lane = lax.broadcasted_iota(jnp.int32, (span, 128), 1)
    first = lane % HEAD_DIM < HEAD_DIM // 2
    lane_out = lax.broadcasted_iota(jnp.int32, (HEAD_DIM, 128), 1)
    block = seqs * HEAD_DIM // n_a
    for s in range(seqs):
        select = jnp.where(row_hs == lane_head * seqs + s, 1.0, 0.0).astype(F32)
        weights = [
            jnp.exp(jnp.dot(suffix[tb], select, precision=HIGH, preferred_element_type=F32))
            for tb in range(2)
        ]
        for c0 in range(0, cols, 128):
            total = None
            for tb in range(2):
                at = pl.ds(s * span, span)
                u = kv[0, tb, at, pl.ds(c0, 128)].astype(F32)
                turned = jnp.where(first, pltpu.roll(u, 128 - 32, 1), pltpu.roll(u, 32, 1))
                spot = pl.ds(tb * span, span)
                rk = u * cos_ref[spot, :] + turned * sin_ref[spot, :]
                weighted = (rk * weights[tb][:, c0:c0 + 128]).astype(jnp.bfloat16)
                term = lax.dot_general(
                    weighted, kv[1, tb, at, pl.ds(c0, 128)], (((0,), (0,)), ((), ())),
                    preferred_element_type=F32,
                )
                total = term if total is None else total + term
            both = jnp.where(lane_out < HEAD_DIM, total[:HEAD_DIM], total[HEAD_DIM:])
            part[pl.ds(s * HEAD_DIM, HEAD_DIM), pl.ds(c0, 128)] = both.astype(jnp.bfloat16)

    def block_of(k):
        return pl.ds(pl.multiple_of(k * block, block), block)

    def rs(k):
        to = lax.rem(a + k, n_a)
        return remote(part.at[block_of(to)], got.at[k], rs_s.at[k], rs_r.at[k], (g, to * 2 + b, tp))

    @pl.loop(1, n_a)
    def _(k):
        rs(k).start()

    @pl.loop(1, n_a)
    def _(k):
        rs(k).wait_recv()

    def gather(k, total):
        return total + got[k].astype(F32)

    reduced = lax.fori_loop(1, n_a, gather, part[block_of(a), :].astype(F32))
    full[b, block_of(a), :] = reduced.astype(jnp.bfloat16)

    def ag(k):
        here = full.at[b, block_of(a)]
        return remote(here, here, ag_s.at[k], ag_r.at[k], (g, lax.rem(a + k, n_a) * 2 + b, tp))

    def ag_in(k):
        here = full.at[b, block_of(lax.rem(a - k + n_a, n_a))]
        return remote(here, here, ag_s.at[k], ag_r.at[k], y_peer)

    def yg(k, bb):
        here = full.at[bb, block_of(lax.rem(a - k + n_a, n_a))]
        return remote(here, here, yg_s.at[k], yg_r.at[k], y_peer)

    @pl.loop(1, n_a)
    def _(k):
        ag(k).start()

    yg(0, b).start()

    @pl.loop(1, n_a)
    def _(k):
        ag_in(k).wait_recv()
        yg(k, b).start()

    @pl.loop(0, n_a)
    def _(k):
        yg(k, ob).wait_recv()

    for c0 in range(0, 2 * cols, 128):
        chunk = pl.ds(c0, 128)
        raws, states = [], []
        for s in range(seqs):
            at = pl.ds(s * HEAD_DIM, HEAD_DIM)
            summed = full[c0 // cols, at, pl.ds(c0 % cols, 128)].astype(F32)
            state = decay[s:s + 1, chunk] * summed + outer[at, chunk]
            raws.append(jnp.sum(qx[at, chunk] * state, axis=0, keepdims=True))
            states.append(state)
        out[chunk, :] = jnp.concatenate(states, axis=0).T
        raw = jnp.concatenate(raws, axis=0)
        center = exact(raw, same_head) * (1.0 / HEAD_DIM)
        off = raw - center
        spread = exact(off * off, same_head) * (1.0 / HEAD_DIM)
        read[:, chunk] = (off * lax.rsqrt(spread + 1e-06) * gain[:, chunk]).astype(jnp.bfloat16)

    @pl.loop(0, n_a)
    def _(k):
        yg(k, b).wait_send()

    @pl.loop(1, n_a)
    def _(k):
        ag(k).wait_send()
        rs(k).wait_send()

    @pl.loop(1, n_sp)
    def _(k):
        tsend(k).wait_send()

    ytok.wait_send()
    yld.wait_send()
    ctok.wait_send()
    for q in range(SUB):
        for m in range(2):
            yw(m, q).wait_send()
        for s in (sp, a * 2 + ob):
            @pl.when(a < n_a - 1)
            def _():
                zsend(s, q, True).wait_send()

            @pl.when(a > 0)
            def _():
                zsend(s, q, False).wait_send()

    @pl.loop(1, n_a)
    def _(d):
        for bb in range(2):
            for q in range(SUB):
                below = (a - d) * 2 + (b if bb == 0 else ob)
                above = (a + d) * 2 + (b if bb == 0 else ob)

                @pl.when(a - d >= 0)
                def _():
                    @pl.when(a < n_a - 1)
                    def _():
                        zsend(below, q, True).wait_send()

                    xsend(below, q).wait_send()

                @pl.when(a + d < n_a)
                def _():
                    @pl.when(a > 0)
                    def _():
                        zsend(above, q, False).wait_send()

                    xsend(above, q).wait_send()


def prompt_states(token_rows, key_weight, value_weight, decays, cos, sin, step, seqs, span, heads, n_sp):
    rows, width = token_rows.shape
    depth, whole = key_weight.shape
    cols = whole // 2
    n_a = n_sp // 2
    hs = heads * seqs
    state_rows = seqs * HEAD_DIM
    dma = pltpu.SemaphoreType.DMA
    bf16 = jnp.bfloat16
    hbm = pl.BlockSpec(memory_space=pl.ANY)
    vmem = pl.BlockSpec(memory_space=pltpu.VMEM)
    return pl.pallas_call(
        functools.partial(kernel, (n_sp, seqs, span, heads)),
        out_shape=(
            jax.ShapeDtypeStruct((whole, state_rows), F32),
            jax.ShapeDtypeStruct((seqs, whole), bf16),
        ),
        in_specs=[hbm] * 6 + [vmem] * 5,
        out_specs=(vmem, vmem),
        scratch_shapes=[
            pltpu.VMEM((2, rows, width), bf16),
            pltpu.VMEM((2, n_sp * depth, cols), bf16),
            pltpu.VMEM((2, 2, rows, cols), bf16),
            pltpu.VMEM((2, rows, cols), F32),
            pltpu.VMEM((2, hs, span), F32),
            pltpu.VMEM((n_sp, 8, 128), F32),
            pltpu.VMEM((state_rows, cols), bf16),
            pltpu.VMEM((n_a, state_rows // n_a, cols), bf16),
            pltpu.VMEM((2, state_rows, cols), bf16),
            pltpu.VMEM((2 * span, 128), F32),
            pltpu.VMEM((2 * span, 128), F32),
            pltpu.VMEM((2, 8, 128), F32),
            pltpu.VMEM((state_rows, whole), F32),
            pltpu.VMEM((state_rows, whole), F32),
            pltpu.VMEM((seqs, whole), F32),
            dma((8,)), dma, dma, dma, dma,
            dma((2, SUB)), dma((2, SUB)),
            dma((n_sp, SUB)), dma((n_sp, SUB)), dma((n_sp, SUB)),
            dma((n_sp, SUB)), dma((n_sp, SUB)),
            dma, dma, dma((n_sp,)), dma((n_sp,)),
            dma((n_a,)), dma((n_a,)), dma((n_a,)), dma((n_a,)), dma((n_a,)), dma((n_a,)),
        ],
        compiler_params=pltpu.CompilerParams(
            collective_id=0, has_side_effects=True, vmem_limit_bytes=56 * 1024 * 1024
        ),
    )(token_rows, key_weight, value_weight, decays, cos, sin, *step)


def position_tables(length):
    half = HEAD_DIM // 2
    inverse = np.float32(10000.0) ** (-np.arange(half, dtype=np.float32) * np.float32(2.0 / HEAD_DIM))
    angles = np.arange(length + 8, dtype=np.float32)[:, None] * inverse[None, :].astype(np.float32)
    cosine = np.cos(angles.astype(np.float64)) * HEAD_DIM ** -0.5
    sine = np.sin(angles.astype(np.float64)) * HEAD_DIM ** -0.5
    cos = np.concatenate([cosine] * 4, axis=-1).astype(np.float32)
    sin = np.concatenate([-sine, sine] * 2, axis=-1).astype(np.float32)
    return cos, sin


def shards(
    tokens, key_weight, value_weight, log_decay, new_query, new_key, new_value, step_decay, norm_gain
):
    seqs, span, width = tokens.shape
    heads = key_weight.shape[1] // HEAD_DIM
    n_sp = lax.axis_size("sp")
    token_rows = tokens.reshape(seqs * span, width)
    decays = log_decay.reshape(heads * seqs, span)
    cos, sin = position_tables(span * n_sp)
    step = (new_query, new_key, new_value, step_decay.T, norm_gain.reshape(1, -1))
    state, read = prompt_states(
        token_rows, key_weight, value_weight, decays, jnp.asarray(cos), jnp.asarray(sin), step,
        seqs, span, heads, n_sp,
    )
    return (state.T.reshape(seqs * HEAD_DIM, heads, HEAD_DIM), read)


def solution(mesh):
    placed = (
        P("gr", "sp", None),
        P("sp", "tp"),
        P("sp", "tp"),
        P("tp", "gr", "sp"),
        P("gr", "tp"),
        P("gr", "tp"),
        P("gr", "tp"),
        P("tp", "gr"),
        P("tp"),
    )
    return jax.shard_map(
        shards,
        mesh=mesh,
        in_specs=placed,
        out_specs=(P("gr", "tp", None), P("gr", "tp")),
        check_vma=False,
    )
```

profile of v0, /device:TPU:0, one launch (start us, length us, event | category | flops | bytes accessed | tf_op | source)
XLA Modules:
  0.0 117.0 jit_solution(16630168108116369539)
XLA Ops:
  0.6 112.7 %shard_map.122 = (f32[1024,256]{1,0:T(8,128)}, bf16[4,1024]{1,0:T(4,128)(2,1)}) custom-call(bf16[512,4096]{1,0:T(8,128)(2,1)} %bitcast.7, bf16[512,1024]{1,0:T(8,128)(2,1)} %kw.1, bf16[512,1024]{1,0:T(8,128)(2,1)} %vw.1, f32[64,128]{1,0:T(8,128)} %bitcast.9, f32[1032,128]{1,0:T(8,128)} %constant.4.clone.cos_tab, f32[1032,128]{1,0:T(8,128)} %constant.5.clone.sin_tab, ...), custom_call_target="tpu_custom_call" | custom-call | tf_op jit(solution)/shard_map/pallas_call | solution.py:447
  113.4 2.3 %copy.15 = f32[256,16,64]{0,2,1:T(8,128)} copy(f32[256,16,64]{0,2,1:T(8,128)} %bitcast.8) | data formatting | bytes 2097152
  115.7 1.3 %copy.16 = bf16[4,1024]{1,0:T(4,128)(2,1)} copy(bf16[4,1024]{1,0:T(4,128)(2,1)} %get-tuple-element.9) | data formatting | bytes 16384
where the time goes:
time: 117 us
  Pallas kernels  113 us (97%)
  local copies, waits for them, and re-layouts  3.59 us (3%)
    pallas_call x1, Pallas kernels, prompt_states(): pl.pallas_call(functools.partial(kernel, (n_sp, seqs, span, heads)), out_...  113 us
    unnamed x2, local copies, waits for them, and re-layouts  3.59 us

commit v1 on v0

v1 whole, which is shorter than its diff:
```python
import functools

import jax
import jax.numpy as jnp
import numpy as np
from jax import lax
from jax.experimental import pallas as pl
from jax.experimental.pallas import tpu as pltpu
from jax.sharding import PartitionSpec as P

HEAD_DIM = 64
GROUPS = 2
MESH = pl.DeviceIdType.MESH
F32 = jnp.float32
HIGH = lax.Precision.HIGHEST


def kernel(
    sizes,
    tok, kw, vw, ld, cos_tab, sin_tab, nq, nk, nv, sd, gain,
    out, read,
    toks, w, lds, tots, wts, own_state, part, got, full, cos_ref, sin_ref, ends, qx, outer, decay, raw_ref,
    l_sem, w_sem, yw_s, yw_r, tok_s, tok_r, core_s, core_r, z_s, z_r, x_s, x_r,
    ld_s, ld_r, tot_s, tot_r, rs_s, rs_r, ag_s, ag_r, yg_s, yg_r,
):
    n_sp, seqs, span, heads = sizes
    n_a = n_sp // 2
    g, sp, tp = lax.axis_index("gr"), lax.axis_index("sp"), lax.axis_index("tp")
    a, b = sp // 2, sp % 2
    ob = 1 - b
    core = tp % 2
    mate = tp + 1 - 2 * core
    rows, width = tok.shape
    depth = kw.shape[0]
    cols = kw.shape[1] // 2
    n_c = cols // 128
    in_group = seqs // GROUPS
    group_rows = in_group * span
    group_state = in_group * HEAD_DIM
    hs = heads * seqs
    peer = a * 2 + ob
    y_peer = (g, peer, tp)
    x_peer = (1 - g, sp, tp)
    core_peer = (g, sp, mate)
    edge = jnp.logical_or(a == 0, a == n_a - 1)
    ahead = jnp.where(a < n_a // 2, 1, -1)

    def lanes(m):
        return pl.ds(m * 128 if isinstance(m, int) else pl.multiple_of(m * 128, 128), 128)

    def columns(side, j):
        return pl.ds(pl.multiple_of(side * cols + j * 128, 128), 128)

    def shard_rows(s):
        return pl.ds(pl.multiple_of(s * depth, depth), depth)

    def own_weight(m, j):
        return pltpu.make_async_copy(
            (kw, vw)[m].at[:, columns(b, j)], w.at[j, shard_rows(sp), lanes(m)], w_sem.at[m, j]
        )

    local = [
        pltpu.make_async_copy(ld, lds.at[b], l_sem.at[0]),
        pltpu.make_async_copy(tok, toks.at[b], l_sem.at[1]),
        pltpu.make_async_copy(cos_tab.at[pl.ds(pl.multiple_of(a * 2 * span, 8), 2 * span)], cos_ref, l_sem.at[2]),
        pltpu.make_async_copy(sin_tab.at[pl.ds(pl.multiple_of(a * 2 * span, 8), 2 * span)], sin_ref, l_sem.at[3]),
        pltpu.make_async_copy(cos_tab.at[pl.ds(n_sp * span, 8)], ends.at[0], l_sem.at[4]),
        pltpu.make_async_copy(sin_tab.at[pl.ds(n_sp * span, 8)], ends.at[1], l_sem.at[5]),
    ]
    for j in range(n_c):
        for m in range(2):
            own_weight(m, j).start()
    for c in local:
        c.start()

    barrier = pltpu.get_barrier_semaphore()

    @pl.loop(1, n_sp)
    def _(k):
        pl.semaphore_signal(barrier, inc=1, device_id=(g, lax.rem(sp + k, n_sp), tp), device_id_type=MESH)

    pl.semaphore_signal(barrier, inc=1, device_id=x_peer, device_id_type=MESH)
    pl.semaphore_signal(barrier, inc=1, device_id=core_peer, device_id_type=MESH)
    pl.semaphore_wait(barrier, n_sp + 1)

    def remote(src, dst, s, r, dev):
        return pltpu.make_async_remote_copy(
            src_ref=src, dst_ref=dst, send_sem=s, recv_sem=r, device_id=dev, device_id_type=MESH
        )

    def yw(m, j):
        return remote(
            (kw, vw)[m].at[:, columns(ob, j)], w.at[j, shard_rows(sp), lanes(m)], yw_s.at[m, j], yw_r.at[m, j], y_peer
        )

    def half_group(h):
        half = group_rows // 2
        return pl.ds(pl.multiple_of(h * group_rows + core * half, half), half)

    def ytok(h):
        return remote(tok.at[half_group(h)], toks.at[b, half_group(h)], tok_s.at[h], tok_r.at[h], y_peer)

    def ytok_in(h):
        here = toks.at[ob, half_group(h)]
        return remote(here, here, tok_s.at[h], tok_r.at[h], y_peer)

    def ctok(h):
        here = toks.at[ob, half_group(h)]
        return remote(here, here, core_s.at[h], core_r.at[h], core_peer)

    yld = remote(ld, lds.at[b], ld_s, ld_r, y_peer)

    early = min(2, n_c)
    soon = min(3, n_c)
    for m in range(2):
        @pl.when(g == m)
        def _():
            for j in range(early):
                yw(m, j).start()
            yld.start()
            for j in range(early):
                yw(1 - m, j).start()
            for j in range(early, soon):
                yw(m, j).start()
            ytok(0).start()
            for j in range(soon, n_c):
                yw(m, j).start()
            for j in range(early, n_c):
                yw(1 - m, j).start()
            for h in range(1, GROUPS):
                ytok(h).start()

    def yw_wait(m_is_g, j):
        for m in range(2):
            @pl.when(g == (m if m_is_g else 1 - m))
            def _():
                yw(m, j).wait_recv()

    def zsend(j, s, t):
        ref = w.at[j, shard_rows(s), lanes(g)]
        return remote(ref, ref, z_s.at[(t + 1) // 2, j, s], z_r.at[j, s], (g, sp + 2 * t, tp))

    def xsend(j, s):
        ref = w.at[j, shard_rows(s), lanes(g)]
        return remote(ref, ref, x_s.at[j, s], x_r.at[j, s], x_peer)

    def xrecv(j, s):
        ref = w.at[j, shard_rows(s), lanes(1 - g)]
        return remote(ref, ref, x_s.at[j, s], x_r.at[j, s], x_peer)

    def exists(place):
        return jnp.logical_and(place >= 0, place < n_a)

    def launch(j, s):
        for t in (-ahead, ahead):
            @pl.when(exists(a + t))
            def _():
                zsend(j, s, t).start()

    def start_chunk(j):
        own_weight(0, j).wait()
        own_weight(1, j).wait()
        launch(j, sp)
        yw_wait(True, j)
        launch(j, peer)

    def zstep(j, d, bb):
        side = b if bb == 0 else ob
        for t in (ahead, -ahead):
            @pl.when(exists(a + t * d))
            def _():
                s = (a + t * d) * 2 + side
                zsend(j, s, -t).wait_recv()

                @pl.when(exists(a - t))
                def _():
                    zsend(j, s, -t).start()

                xsend(j, s).start()

    def gather_x(j):
        yw_wait(False, j)

        @pl.loop(0, n_sp)
        def _(s):
            @pl.when(s // 2 != a)
            def _():
                xrecv(j, s).wait_recv()

    start_chunk(0)

    def tsend(k):
        return remote(tots.at[sp], tots.at[sp], tot_s.at[k], tot_r.at[k], (g, lax.rem(sp + k, n_sp), tp))

    for c in local:
        c.wait()
    raw_ref[...] = jnp.zeros(raw_ref.shape, F32)
    tots[sp] = jnp.zeros(tots.shape[1:], F32)
    tots[sp, :, 0:hs] = lax.dot_general(
        jnp.ones((8, span), F32), lds[b], (((1,), (1,)), ((), ())), precision=HIGH, preferred_element_type=F32
    )

    lanes_at = lax.broadcasted_iota(jnp.int32, (HEAD_DIM, 128), 1)
    subs_at = lax.broadcasted_iota(jnp.int32, (HEAD_DIM, 128), 0)
    diagonal = lanes_at % HEAD_DIM == subs_at
    same_head = jnp.where(
        lax.broadcasted_iota(jnp.int32, (128, 128), 0) // HEAD_DIM
        == lax.broadcasted_iota(jnp.int32, (128, 128), 1) // HEAD_DIM, 1.0, 0.0
    ).astype(F32)

    def exact(x, y):
        return jnp.dot(x, y, precision=HIGH, preferred_element_type=F32)

    def at_end(u):
        low = lax.broadcasted_iota(jnp.int32, u.shape, 1) % HEAD_DIM < HEAD_DIM // 2
        turned = jnp.where(low, pltpu.roll(u, 128 - 32, 1), pltpu.roll(u, 32, 1))
        return u * ends[0, 0:1, :] + turned * ends[1, 0:1, :]

    head_lane = lax.broadcasted_iota(jnp.int32, (heads, 2 * cols), 1) // HEAD_DIM
    head_row = lax.broadcasted_iota(jnp.int32, (heads, 2 * cols), 0)
    spread_heads = jnp.where(head_lane == head_row, 1.0, 0.0).astype(F32)
    decay[...] = jnp.exp(exact(sd[...], spread_heads))

    @pl.loop(1, n_sp)
    def _(k):
        tsend(k).start()

    def new_token(c0):
        chunk = pl.ds(c0, 128)
        query = at_end(nq[:, chunk].astype(F32)) * HEAD_DIM ** 0.5
        key_new = at_end(nk[:, chunk].astype(F32))
        value_new = nv[:, chunk].astype(F32)
        for s in range(seqs):
            at = pl.ds(s * HEAD_DIM, HEAD_DIM)
            qx[at, chunk] = exact(jnp.where(diagonal, query[s:s + 1], 0.0), same_head)
            column = exact(jnp.where(diagonal, key_new[s:s + 1], 0.0), same_head)
            outer[at, chunk] = column * value_new[s:s + 1]

    def weigh():
        yld.wait_recv()

        @pl.loop(1, n_sp)
        def _(k):
            tsend(k).wait_recv()

        pos_t = lax.broadcasted_iota(jnp.int32, (span, span), 0)
        pos_u = lax.broadcasted_iota(jnp.int32, (span, span), 1)
        later_mask = jnp.where(pos_u > pos_t, 1.0, 0.0).astype(F32)
        row_hs = lax.broadcasted_iota(jnp.int32, (hs, cols), 0)
        lane_head = lax.broadcasted_iota(jnp.int32, (hs, cols), 1) // HEAD_DIM + b * (heads // 2)
        for tb in range(2):
            inside = lax.dot_general(
                later_mask, lds[tb], (((1,), (1,)), ((), ())), precision=HIGH, preferred_element_type=F32
            )
            index = a * 2 + tb

            def add(k, total):
                return total + jnp.where(k > index, tots[k], 0.0)

            after = lax.fori_loop(0, n_sp, add, jnp.zeros(tots.shape[1:], F32))
            suffix = inside + after[0:1, :hs]
            for s in range(seqs):
                select = jnp.where(row_hs == lane_head * seqs + s, 1.0, 0.0).astype(F32)
                wts[tb, s] = jnp.exp(jnp.dot(suffix, select, precision=HIGH, preferred_element_type=F32))

    lane = lax.broadcasted_iota(jnp.int32, (span, 128), 1)
    first = lane % HEAD_DIM < HEAD_DIM // 2
    lane_out = lax.broadcasted_iota(jnp.int32, (HEAD_DIM, 128), 1)

    def states(tb, h, j):
        at = pl.ds(pl.multiple_of(h * group_rows, group_rows), group_rows)
        prod = jnp.dot(toks[tb, at, :], w[j], preferred_element_type=F32)
        keys = prod[:, :128].astype(jnp.bfloat16).astype(F32)
        values = prod[:, 128:].astype(jnp.bfloat16)
        spot = pl.ds(pl.multiple_of(tb * span, span), span)
        result = []
        for i in range(in_group):
            u = keys[i * span:(i + 1) * span]
            turned = jnp.where(first, pltpu.roll(u, 128 - 32, 1), pltpu.roll(u, 32, 1))
            rk = u * cos_ref[spot, :] + turned * sin_ref[spot, :]
            weighted = (rk * wts[tb, h * in_group + i, :, pl.ds(j * 128, 128)]).astype(jnp.bfloat16)
            term = lax.dot_general(
                weighted, values[i * span:(i + 1) * span], (((0,), (0,)), ((), ())), preferred_element_type=F32
            )
            result.append(jnp.where(lane_out < HEAD_DIM, term[:HEAD_DIM], term[HEAD_DIM:]))
        return jnp.concatenate(result, axis=0)

    def own(j):
        @pl.loop(0, GROUPS)
        def _(h):
            own_state[h, j] = states(b, h, j)

    def reducer(h):
        return n_a // 2 - 1 + h

    def rs(h, j):
        to = reducer(h)
        return remote(part.at[h, j], got.at[a, j], rs_s.at[h, j], rs_r.at[a, j], (g, to * 2 + b, tp))

    def rs_in(src, h, j):
        return remote(part.at[h, j], got.at[src, j], rs_s.at[h, j], rs_r.at[src, j], y_peer)

    def partner(h, j):
        part[h, j] = (own_state[h, j] + states(ob, h, j)).astype(jnp.bfloat16)

        @pl.when(a != reducer(h))
        def _():
            rs(h, j).start()

    def ag(h, j, to):
        here = full.at[b, h, j]
        return remote(here, here, ag_s.at[j, to], ag_r.at[h, j], (g, to * 2 + b, tp))

    def yg(h, j, side):
        here = full.at[side, h, j]
        return remote(here, here, yg_s.at[h, j], yg_r.at[h, j], y_peer)

    def reduce(h, j):
        @pl.when(a == reducer(h))
        def _():
            def add(k, total):
                src = lax.rem(a + k, n_a)
                rs_in(src, h, j).wait_recv()
                return total + got[src, j].astype(F32)

            total = lax.fori_loop(1, n_a, add, part[h, j].astype(F32))
            full[b, h, j] = total.astype(jnp.bfloat16)

            @pl.loop(1, n_a)
            def _(k):
                ag(h, j, lax.rem(a + k, n_a)).start()

            yg(h, j, b).start()

    def collect(h, j):
        @pl.when(a != reducer(h))
        def _():
            ag(h, j, a).wait_recv()
            yg(h, j, b).start()

    def finish(side, h, j):
        chunk = columns(side, j)
        raws, done = [], []
        for i in range(in_group):
            s = h * in_group + i
            at = pl.ds(s * HEAD_DIM, HEAD_DIM)
            summed = full[side, h, j, i * HEAD_DIM:(i + 1) * HEAD_DIM, :].astype(F32)
            state = decay[s:s + 1, chunk] * summed + outer[at, chunk]
            raws.append(jnp.sum(qx[at, chunk] * state, axis=0, keepdims=True))
            done.append(state)
        out[chunk, h * group_state:(h + 1) * group_state] = jnp.concatenate(done, axis=0).T
        raw_ref[side * n_c + j, h * in_group:(h + 1) * in_group, :] = jnp.concatenate(raws, axis=0)

    def tokens_in(h):
        ytok_in(h).wait_recv()
        ctok(h).start()

    new_chunks = list(range(0, 2 * cols, 128))
    last = n_c - 1
    for j in range(n_c):
        if j > 0:
            @pl.when(jnp.logical_not(edge))
            def _():
                start_chunk(j)

        for step in range(6):
            zstep(j, step // 2 + 1, step % 2)
            if step == 2 and j < last:
                @pl.when(edge)
                def _():
                    start_chunk(j + 1)
            if j == 0:
                for c0 in new_chunks[step::4] if step < 4 else ():
                    new_token(c0)
                if step == 3:
                    weigh()
            else:
                if step == 2:
                    gather_x(j - 1)
                    own(j - 1)
                if j == last - 1 and step == 3:
                    tokens_in(0)
                if j == last - 1 and step == 4:
                    ctok(0).wait_recv()
                    for k in range(last - 1):
                        partner(0, k)
                if j == last and step == 3:
                    if last < 2:
                        tokens_in(0)
                        ctok(0).wait_recv()
                    partner(0, last - 1)
                if j == last and step == 4:
                    for k in range(last - 1):
                        reduce(0, k)
                if j == last and step == 5:
                    for k in range(last - 1):
                        collect(0, k)

        @pl.loop(4, n_a)
        def _(d):
            for bb in range(2):
                zstep(j, d, bb)

    tokens_in(1)
    reduce(0, last - 1)
    ctok(1).wait_recv()
    for j in range(last):
        partner(1, j)
    collect(0, last - 1)
    gather_x(last)
    own(last)
    for h in range(GROUPS):
        partner(h, last)
    for j in range(last):
        reduce(1, j)
    for j in range(last):
        collect(1, j)
    for h in range(GROUPS):
        reduce(h, last)
    for j in range(last):
        finish(b, 0, j)
        yg(0, j, ob).wait_recv()
        finish(ob, 0, j)
    for j in range(last):
        finish(b, 1, j)
        yg(1, j, ob).wait_recv()
        finish(ob, 1, j)
    for h in range(GROUPS):
        collect(h, last)
    for h in range(GROUPS):
        finish(b, h, last)
    for h in range(GROUPS):
        yg(h, last, ob).wait_recv()
        finish(ob, h, last)

    count = 2 * n_c
    raw = jnp.concatenate([raw_ref[c] for c in range(count)], axis=0)
    off = raw - exact(raw, same_head) * (1.0 / HEAD_DIM)
    spread = exact(off * off, same_head) * (1.0 / HEAD_DIM)
    normed = off * lax.rsqrt(spread + 1e-06)
    for c in range(count):
        chunk = pl.ds(c * 128, 128)
        read[:, chunk] = (normed[c * 8:c * 8 + seqs] * gain[:, chunk]).astype(jnp.bfloat16)

    for h in range(GROUPS):
        for j in range(n_c):
            yg(h, j, b).wait_send()

            @pl.when(a != reducer(h))
            def _():
                rs(h, j).wait_send()

            @pl.when(a == reducer(h))
            def _():
                @pl.loop(1, n_a)
                def _(k):
                    ag(h, j, lax.rem(a + k, n_a)).wait_send()

        ytok(h).wait_send()
        ctok(h).wait_send()

    @pl.loop(1, n_sp)
    def _(k):
        tsend(k).wait_send()

    yld.wait_send()
    for j in range(n_c):
        for m in range(2):
            yw(m, j).wait_send()
        for s in (sp, peer):
            for t in (-ahead, ahead):
                @pl.when(exists(a + t))
                def _():
                    zsend(j, s, t).wait_send()

    @pl.loop(0, n_c)
    def _(j):
        @pl.loop(1, n_a)
        def _(d):
            for side in (b, ob):
                for t in (ahead, -ahead):
                    @pl.when(exists(a + t * d))
                    def _():
                        s = (a + t * d) * 2 + side

                        @pl.when(exists(a - t))
                        def _():
                            zsend(j, s, -t).wait_send()

                        xsend(j, s).wait_send()


def prompt_states(token_rows, key_weight, value_weight, decays, cos, sin, step, seqs, span, heads, n_sp):
    rows, width = token_rows.shape
    depth, whole = key_weight.shape
    cols = whole // 2
    n_c = cols // 128
    n_a = n_sp // 2
    hs = heads * seqs
    state_rows = seqs * HEAD_DIM
    group_state = state_rows // GROUPS
    dma = pltpu.SemaphoreType.DMA
    bf16 = jnp.bfloat16
    hbm = pl.BlockSpec(memory_space=pl.ANY)
    vmem = pl.BlockSpec(memory_space=pltpu.VMEM)
    operands = (token_rows, key_weight, value_weight, decays, cos, sin, *step)
    return pl.pallas_call(
        functools.partial(kernel, (n_sp, seqs, span, heads)),
        out_shape=(
            pltpu.VMEM((whole, state_rows), F32),
            pltpu.VMEM((seqs, whole), bf16),
        ),
        in_specs=[hbm] * 6 + [vmem] * 5,
        out_specs=(vmem, vmem),
        scratch_shapes=[
            pltpu.VMEM((2, rows, width), bf16),
            pltpu.VMEM((n_c, n_sp * depth, 256), bf16),
            pltpu.VMEM((2, hs, span), F32),
            pltpu.VMEM((n_sp, 8, 128), F32),
            pltpu.VMEM((2, seqs, span, cols), F32),
            pltpu.VMEM((GROUPS, n_c, group_state, 128), F32),
            pltpu.VMEM((GROUPS, n_c, group_state, 128), bf16),
            pltpu.VMEM((n_a, n_c, group_state, 128), bf16),
            pltpu.VMEM((2, GROUPS, n_c, group_state, 128), bf16),
            pltpu.VMEM((2 * span, 128), F32),
            pltpu.VMEM((2 * span, 128), F32),
            pltpu.VMEM((2, 8, 128), F32),
            pltpu.VMEM((state_rows, whole), F32),
            pltpu.VMEM((state_rows, whole), F32),
            pltpu.VMEM((seqs, whole), F32),
            pltpu.VMEM((2 * n_c, 8, 128), F32),
            dma((6,)), dma((2, n_c)), dma((2, n_c)), dma((2, n_c)),
            dma((GROUPS,)), dma((GROUPS,)), dma((GROUPS,)), dma((GROUPS,)),
            dma((2, n_c, n_sp)), dma((n_c, n_sp)), dma((n_c, n_sp)), dma((n_c, n_sp)),
            dma, dma, dma((n_sp,)), dma((n_sp,)),
            dma((GROUPS, n_c)), dma((n_a, n_c)), dma((n_c, n_a)), dma((GROUPS, n_c)),
            dma((GROUPS, n_c)), dma((GROUPS, n_c)),
        ],
        compiler_params=pltpu.CompilerParams(
            collective_id=0, has_side_effects=True, vmem_limit_bytes=40 * 1024 * 1024
        ),
    )(*[pltpu.with_memory_space_constraint(v, pltpu.HBM) for v in operands])


def position_tables(length):
    half = HEAD_DIM // 2
    inverse = np.float32(10000.0) ** (-np.arange(half, dtype=np.float32) * np.float32(2.0 / HEAD_DIM))
    angles = np.arange(length + 8, dtype=np.float32)[:, None] * inverse[None, :].astype(np.float32)
    cosine = np.cos(angles.astype(np.float64)) * HEAD_DIM ** -0.5
    sine = np.sin(angles.astype(np.float64)) * HEAD_DIM ** -0.5
    cos = np.concatenate([cosine] * 4, axis=-1).astype(np.float32)
    sin = np.concatenate([-sine, sine] * 2, axis=-1).astype(np.float32)
    return cos, sin


def shards(
    tokens, key_weight, value_weight, log_decay, new_query, new_key, new_value, step_decay, norm_gain
):
    seqs, span, width = tokens.shape
    heads = key_weight.shape[1] // HEAD_DIM
    n_sp = lax.axis_size("sp")
    token_rows = tokens.reshape(seqs * span, width)
    decays = log_decay.reshape(heads * seqs, span)
    cos, sin = position_tables(span * n_sp)
    step = (new_query, new_key, new_value, step_decay.T, norm_gain.reshape(1, -1))
    state, read = prompt_states(
        token_rows, key_weight, value_weight, decays, jnp.asarray(cos), jnp.asarray(sin), step,
        seqs, span, heads, n_sp,
    )
    return (state.T.reshape(seqs * HEAD_DIM, heads, HEAD_DIM), read)


def solution(mesh):
    placed = (
        P("gr", "sp", None),
        P("sp", "tp"),
        P("sp", "tp"),
        P("tp", "gr", "sp"),
        P("gr", "tp"),
        P("gr", "tp"),
        P("gr", "tp"),
        P("tp", "gr"),
        P("tp"),
    )
    return jax.shard_map(
        shards,
        mesh=mesh,
        in_specs=placed,
        out_specs=(P("gr", "tp", None), P("gr", "tp")),
        check_vma=False,
    )
```

time: 117 us -> 161 us (1.38)
  Pallas kernels: 113 us -> 159 us
  local copies, waits for them, and re-layouts: 3.59 us -> 1.57 us
    pallas_call x1, Pallas kernels: 113 us -> 159 us  [prompt_states(): pl.pallas_call(functools.partial(kernel, (n_sp, seqs, span, heads)), out_...]
    unnamed x2, local copies, waits for them, and re-layouts: 3.59 us -> 1.57 us
where the time goes in v1:
time: 161 us
  Pallas kernels  159 us (99%)
    pallas_call x1, Pallas kernels, prompt_states(): pl.pallas_call(functools.partial(kernel, (n_sp, seqs, span, heads)), out_...  159 us

profile of v1, /device:TPU:0, one launch (start us, length us, event | category | flops | bytes accessed | tf_op | source)
XLA Modules:
  0.0 160.7 jit_solution(592207189521076132)
XLA Ops:
  0.6 158.5 %shard_map.122 = (f32[1024,256]{1,0:T(8,128)S(1)}, bf16[4,1024]{1,0:T(4,128)(2,1)S(1)}) custom-call(bf16[512,4096]{1,0:T(8,128)(2,1)} %bitcast.8, bf16[512,1024]{1,0:T(8,128)(2,1)} %kw.1, bf16[512,1024]{1,0:T(8,128)(2,1)} %vw.1, f32[64,128]{1,0:T(8,128)} %bitcast.9, f32[1032,128]{1,0:T(8,128)} %constant.4.clone.cos_tab, f32[1032,128]{1,0:T(8,128)} %constant.5.clone.sin_tab, ...), custom_call_target="tpu_custom_call" | custom-call | tf_op jit(solution)/shard_map/pallas_call | solution.py:507
  159.2 1.0 copy.15
  160.1 0.6 copy.16

commit v2 on v1

v2 whole, which is shorter than its diff:
```python
import functools

import jax
import jax.numpy as jnp
import numpy as np
from jax import lax
from jax.experimental import pallas as pl
from jax.experimental.pallas import tpu as pltpu
from jax.sharding import PartitionSpec as P

HEAD_DIM = 64
PAIR = 2
MESH = pl.DeviceIdType.MESH
F32 = jnp.float32
HIGH = lax.Precision.HIGHEST


def kernel(
    sizes,
    tok, kw, vw, ld, cos_tab, sin_tab, nq, nk, nv, sd, gain,
    out, read,
    staged, read_at, toks, w, lds, tots, wts, own_state, part, got, full, cos_ref, sin_ref, ends, qx, outer, decay, raw_ref, acc,
    l_sem, w_sem, yw_s, yw_r, tok_s, tok_r, core_s, core_r, z_s, z_r, x_s, x_r,
    ld_s, ld_r, tot_s, tot_r, rs_s, rs_r, ag_s, ag_r, yg_s, yg_r, ac_s, out_sem,
):
    n_sp, seqs, span, heads = sizes
    n_a = n_sp // 2
    g, sp, tp = lax.axis_index("gr"), lax.axis_index("sp"), lax.axis_index("tp")
    a, b = sp // 2, sp % 2
    ob = 1 - b
    core = tp % 2
    mate = tp + 1 - 2 * core
    rows, width = tok.shape
    depth = kw.shape[0]
    cols = kw.shape[1] // 2
    n_c = cols // 128
    last = n_c - 1
    pair_rows = PAIR * span
    pair_state = PAIR * HEAD_DIM
    hs = heads * seqs
    peer = a * 2 + ob
    y_peer = (g, peer, tp)
    x_peer = (1 - g, sp, tp)
    core_peer = (g, sp, mate)
    edge = jnp.logical_or(a == 0, a == n_a - 1)
    ahead = jnp.where(a < n_a // 2, 1, -1)

    def lanes(m):
        return pl.ds(m * 128 if isinstance(m, int) else pl.multiple_of(m * 128, 128), 128)

    def columns(side, j):
        return pl.ds(pl.multiple_of(side * cols + j * 128, 128), 128)

    def shard_rows(s):
        return pl.ds(pl.multiple_of(s * depth, depth), depth)

    def own_weight(m, j):
        return pltpu.make_async_copy(
            (kw, vw)[m].at[:, columns(b, j)], w.at[j, shard_rows(sp), lanes(m)], w_sem.at[j]
        )

    local = [
        pltpu.make_async_copy(ld, lds.at[b], l_sem.at[0]),
        pltpu.make_async_copy(tok, toks.at[b], l_sem.at[1]),
        pltpu.make_async_copy(cos_tab.at[pl.ds(pl.multiple_of(a * 2 * span, 8), 2 * span)], cos_ref, l_sem.at[2]),
        pltpu.make_async_copy(sin_tab.at[pl.ds(pl.multiple_of(a * 2 * span, 8), 2 * span)], sin_ref, l_sem.at[3]),
        pltpu.make_async_copy(cos_tab.at[pl.ds(n_sp * span, 8)], ends.at[0], l_sem.at[4]),
        pltpu.make_async_copy(sin_tab.at[pl.ds(n_sp * span, 8)], ends.at[1], l_sem.at[5]),
    ]
    for j in range(n_c):
        for m in range(2):
            own_weight(m, j).start()
    for c in local:
        c.start()

    barrier = pltpu.get_barrier_semaphore()

    @pl.loop(1, n_sp)
    def _(k):
        pl.semaphore_signal(barrier, inc=1, device_id=(g, lax.rem(sp + k, n_sp), tp), device_id_type=MESH)

    pl.semaphore_signal(barrier, inc=1, device_id=x_peer, device_id_type=MESH)
    pl.semaphore_signal(barrier, inc=1, device_id=core_peer, device_id_type=MESH)
    pl.semaphore_wait(barrier, n_sp + 1)

    def remote(src, dst, s, r, dev):
        return pltpu.make_async_remote_copy(
            src_ref=src, dst_ref=dst, send_sem=s, recv_sem=r, device_id=dev, device_id_type=MESH
        )

    def drain(ref, sem):
        pltpu.make_async_copy(ref, ref, sem).wait()

    def yw(m, j):
        return remote(
            (kw, vw)[m].at[:, columns(ob, j)], w.at[j, shard_rows(sp), lanes(m)], yw_s, yw_r.at[m, j], y_peer
        )

    def half_prompt(s):
        half = span // 2
        return pl.ds(pl.multiple_of(s * span + core * half, half), half)

    def ytok(h):
        return remote(tok.at[half_prompt(h)], toks.at[b, half_prompt(h)], tok_s, tok_r.at[h], y_peer)

    def ytok_in(h):
        here = toks.at[ob, half_prompt(h)]
        return remote(here, here, tok_s, tok_r.at[h], y_peer)

    def ctok(h):
        here = toks.at[ob, half_prompt(h)]
        return remote(here, here, core_s, core_r.at[h], core_peer)

    yld = remote(ld, lds.at[b], ld_s, ld_r, y_peer)

    early = min(2, n_c)
    soon = min(3, n_c)
    for m in range(2):
        @pl.when(g == m)
        def _():
            for j in range(early):
                yw(m, j).start()
            yld.start()
            for j in range(early):
                yw(1 - m, j).start()
            for j in range(early, soon):
                yw(m, j).start()
            for h in range(seqs // 2):
                ytok(h).start()
            for j in range(soon, n_c):
                yw(m, j).start()
            for j in range(early, last):
                yw(1 - m, j).start()
            for h in range(seqs // 2, seqs):
                ytok(h).start()
            for j in range(max(early, last), n_c):
                yw(1 - m, j).start()

    def yw_wait(m_is_g, j):
        for m in range(2):
            @pl.when(g == (m if m_is_g else 1 - m))
            def _():
                yw(m, j).wait_recv()

    def zsend(j, s, t):
        ref = w.at[j, shard_rows(s), lanes(g)]
        return remote(ref, ref, z_s.at[(t + 1) // 2], z_r.at[j, s], (g, sp + 2 * t, tp))

    def xsend(j, s):
        ref = w.at[j, shard_rows(s), lanes(g)]
        return remote(ref, ref, x_s, x_r.at[j if j < last else last + s // 2], x_peer)

    def exists(place):
        return jnp.logical_and(place >= 0, place < n_a)

    def launch(j, s):
        for t in (-ahead, ahead):
            @pl.when(exists(a + t))
            def _():
                zsend(j, s, t).start()

    def start_own(j):
        drain(w.at[j, shard_rows(sp)], w_sem.at[j])
        launch(j, sp)

    def start_chunk(j):
        if j >= early:
            start_own(j)
        yw_wait(True, j)
        launch(j, peer)

    def zstep(j, d, bb):
        side = b if bb == 0 else ob
        for t in (ahead, -ahead):
            @pl.when(exists(a + t * d))
            def _():
                s = (a + t * d) * 2 + side
                zsend(j, s, -t).wait_recv()

                @pl.when(exists(a - t))
                def _():
                    zsend(j, s, -t).start()

                xsend(j, s).start()

    def gather_x(j):
        yw_wait(False, j)
        drain(w.at[j, pl.ds(0, 2 * (n_a - 1) * depth), lanes(0)], x_r.at[j])

    for j in range(early):
        start_own(j)
    start_chunk(0)

    def tsend(k):
        return remote(tots.at[a], tots.at[a], tot_s, tot_r.at[k], (g, lax.rem(a + k, n_a) * 2 + b, tp))

    for c in local:
        c.wait()
    raw_ref[...] = jnp.zeros(raw_ref.shape, F32)
    tots[a] = jnp.zeros(tots.shape[1:], F32)

    def shard_total(tb):
        return lax.dot_general(
            jnp.ones((8, span), F32), lds[tb], (((1,), (1,)), ((), ())), precision=HIGH, preferred_element_type=F32
        )

    def total():
        yld.wait_recv()
        tots[a, :, 0:hs] = shard_total(0) + shard_total(1)

        @pl.loop(1, n_a)
        def _(k):
            tsend(k).start()

    lanes_at = lax.broadcasted_iota(jnp.int32, (HEAD_DIM, 128), 1)
    subs_at = lax.broadcasted_iota(jnp.int32, (HEAD_DIM, 128), 0)
    diagonal = lanes_at % HEAD_DIM == subs_at
    same_head = jnp.where(
        lax.broadcasted_iota(jnp.int32, (128, 128), 0) // HEAD_DIM
        == lax.broadcasted_iota(jnp.int32, (128, 128), 1) // HEAD_DIM, 1.0, 0.0
    ).astype(F32)

    def exact(x, y):
        return jnp.dot(x, y, precision=HIGH, preferred_element_type=F32)

    def at_end(u):
        low = lax.broadcasted_iota(jnp.int32, u.shape, 1) % HEAD_DIM < HEAD_DIM // 2
        turned = jnp.where(low, pltpu.roll(u, 128 - 32, 1), pltpu.roll(u, 32, 1))
        return u * ends[0, 0:1, :] + turned * ends[1, 0:1, :]

    head_lane = lax.broadcasted_iota(jnp.int32, (heads, 2 * cols), 1) // HEAD_DIM
    head_row = lax.broadcasted_iota(jnp.int32, (heads, 2 * cols), 0)
    spread_heads = jnp.where(head_lane == head_row, 1.0, 0.0).astype(F32)
    decay[...] = jnp.exp(exact(sd[...], spread_heads))

    def new_token(c0):
        chunk = pl.ds(c0, 128)
        query = at_end(nq[:, chunk].astype(F32)) * HEAD_DIM ** 0.5
        key_new = at_end(nk[:, chunk].astype(F32))
        value_new = nv[:, chunk].astype(F32)
        for s in range(seqs):
            at = pl.ds(s * HEAD_DIM, HEAD_DIM)
            qx[at, chunk] = exact(jnp.where(diagonal, query[s:s + 1], 0.0), same_head)
            column = exact(jnp.where(diagonal, key_new[s:s + 1], 0.0), same_head)
            outer[at, chunk] = column * value_new[s:s + 1]

    def weigh():
        @pl.loop(1, n_a)
        def _(k):
            tsend(k).wait_recv()

        pos_t = lax.broadcasted_iota(jnp.int32, (span, span), 0)
        pos_u = lax.broadcasted_iota(jnp.int32, (span, span), 1)
        later_mask = jnp.where(pos_u > pos_t, 1.0, 0.0).astype(F32)
        row_hs = lax.broadcasted_iota(jnp.int32, (hs, cols), 0)
        lane_head = lax.broadcasted_iota(jnp.int32, (hs, cols), 1) // HEAD_DIM + b * (heads // 2)

        def add(k, total):
            return total + jnp.where(k > a, tots[k], 0.0)

        after = lax.fori_loop(0, n_a, add, jnp.zeros(tots.shape[1:], F32))
        for tb in range(2):
            inside = lax.dot_general(
                later_mask, lds[tb], (((1,), (1,)), ((), ())), precision=HIGH, preferred_element_type=F32
            )
            suffix = inside + after[0:1, :hs]
            if tb == 0:
                suffix = suffix + shard_total(1)[0:1]
            for s in range(seqs):
                select = jnp.where(row_hs == lane_head * seqs + s, 1.0, 0.0).astype(F32)
                wts[tb, s] = jnp.exp(jnp.dot(suffix, select, precision=HIGH, preferred_element_type=F32))

    lane = lax.broadcasted_iota(jnp.int32, (span, 128), 1)
    first = lane % HEAD_DIM < HEAD_DIM // 2
    lane_out = lax.broadcasted_iota(jnp.int32, (HEAD_DIM, 128), 1)

    def states(tb, s, n, j):
        at = pl.ds(pl.multiple_of(s * span, span), n * span)
        return contract(jnp.dot(toks[tb, at, :], w[j], preferred_element_type=F32), tb, s, n, j)

    def contract(prod, tb, s, n, j):
        keys = prod[:, :128].astype(jnp.bfloat16).astype(F32)
        values = prod[:, 128:].astype(jnp.bfloat16)
        spot = pl.ds(pl.multiple_of(tb * span, span), span)
        result = []
        for i in range(n):
            u = keys[i * span:(i + 1) * span]
            turned = jnp.where(first, pltpu.roll(u, 128 - 32, 1), pltpu.roll(u, 32, 1))
            rk = u * cos_ref[spot, :] + turned * sin_ref[spot, :]
            weighted = (rk * wts[tb, s + i, :, pl.ds(j * 128, 128)]).astype(jnp.bfloat16)
            term = lax.dot_general(
                weighted, values[i * span:(i + 1) * span], (((0,), (0,)), ((), ())), preferred_element_type=F32
            )
            result.append(jnp.where(lane_out < HEAD_DIM, term[:HEAD_DIM], term[HEAD_DIM:]))
        return result

    def accumulate(place, fresh=False):
        rows_at = pl.ds(pl.multiple_of(place * 2 * depth, 2 * depth), 2 * depth)
        for k, tb in enumerate((b, ob)):
            for r in range(0, rows, pair_rows):
                new = jnp.dot(
                    toks[tb, r:r + pair_rows, rows_at], w[last, rows_at, :], preferred_element_type=F32
                )
                acc[k, r:r + pair_rows] = new if fresh else acc[k, r:r + pair_rows] + new

    def take(d):
        for t in (ahead, -ahead):
            @pl.when(exists(a + t * d))
            def _():
                drain(w.at[last, pl.ds(0, 2 * depth), lanes(0)], x_r.at[last + a + t * d])
                accumulate(a + t * d)

    def own(j):
        @pl.loop(0, seqs // PAIR)
        def _(p):
            for i, state in enumerate(states(b, p * PAIR, PAIR, j)):
                own_state[p * PAIR + i, j] = state

    def reducer(s):
        return n_a // 2 - 1 + s % 2

    def rs(s, j):
        to = reducer(s)
        return remote(part.at[s, j], got.at[a, s // 2, j], rs_s.at[s % 2], rs_r.at[s // 2, j], (g, to * 2 + b, tp))

    def partner(s, n, j):
        for i, state in enumerate(states(ob, s, n, j)):
            part[s + i, j] = (own_state[s + i, j] + state).astype(jnp.bfloat16)
        for i in range(n):
            rs_start(s + i, j)

    def rs_start(s, j):
        @pl.when(a != reducer(s))
        def _():
            rs(s, j).start()

    def ag(s, j, to):
        here = full.at[b, s, j]
        return remote(here, here, ag_s, ag_r.at[s, j], (g, to * 2 + b, tp))

    def direct(s, j):
        return s == seqs - 1 or j == last

    def across(s, j, to):
        here = full.at[b, s, j]
        return remote(here, here, ac_s.at[0 if j == last else 1], yg_r.at[s, j], (g, to * 2 + ob, tp))

    def yg(s, j, side):
        here = full.at[side, s, j]
        return remote(here, here, yg_s, yg_r.at[s, j], y_peer)

    def reduce(s, j):
        @pl.when(a == reducer(s))
        def _():
            drain(got.at[pl.ds(0, n_a - 1), s // 2, j], rs_r.at[s // 2, j])

            def add(k, total):
                return total + got[lax.rem(a + k, n_a), s // 2, j].astype(F32)

            total = lax.fori_loop(1, n_a, add, part[s, j].astype(F32))
            full[b, s, j] = total.astype(jnp.bfloat16)

            @pl.loop(1, n_a)
            def _(k):
                to = lax.rem(a + k, n_a)
                if direct(s, j):
                    across(s, j, to).start()
                ag(s, j, to).start()

            if direct(s, j):
                across(s, j, a).start()
            else:
                yg(s, j, b).start()

    def collect(s, j):
        @pl.when(a != reducer(s))
        def _():
            ag(s, j, a).wait_recv()
            if not direct(s, j):
                yg(s, j, b).start()

    def finish(side, p, j):
        chunk = columns(side, j)
        raws, done = [], []
        for i in range(PAIR):
            s = p * PAIR + i
            at = pl.ds(s * HEAD_DIM, HEAD_DIM)
            state = decay[s:s + 1, chunk] * full[side, s, j].astype(F32) + outer[at, chunk]
            raws.append(jnp.sum(qx[at, chunk] * state, axis=0, keepdims=True))
            done.append(state)
        staged[chunk, p * pair_state:(p + 1) * pair_state] = jnp.concatenate(done, axis=0).T
        raw_ref[side * n_c + j, p * PAIR:(p + 1) * PAIR, :] = jnp.concatenate(raws, axis=0)

    def put(side, j):
        return pltpu.make_async_copy(staged.at[columns(side, j)], out.at[columns(side, j)], out_sem)

    def tokens_in(s):
        ytok_in(s).wait_recv()
        ctok(s).start()

    def normalize(chunks):
        if not chunks:
            return
        raw = jnp.concatenate([raw_ref[c] for c in chunks], axis=0)
        off = raw - exact(raw, same_head) * (1.0 / HEAD_DIM)
        spread = exact(off * off, same_head) * (1.0 / HEAD_DIM)
        normed = off * lax.rsqrt(spread + 1e-06)
        for i, c in enumerate(chunks):
            chunk = pl.ds(c * 128, 128)
            read_at[:, chunk] = (normed[i * 8:i * 8 + seqs] * gain[:, chunk]).astype(jnp.bfloat16)

    new_chunks = list(range(0, 2 * cols, 128))
    for j in range(n_c):
        if j > 0:
            @pl.when(jnp.logical_not(edge))
            def _():
                start_chunk(j)

        for step in range(6):
            zstep(j, step // 2 + 1, step % 2)
            if step == 2 and j < last:
                @pl.when(edge)
                def _():
                    start_chunk(j + 1)
            if j == 0:
                for c0 in new_chunks[step::4] if step < 4 else ():
                    new_token(c0)
                if step == 3:
                    total()
            else:
                if j == 1 and step == 1:
                    weigh()
                if step == 2:
                    gather_x(j - 1)
                    own(j - 1)
                if j == last - 1 and step == 3:
                    for s in range(seqs // 2):
                        tokens_in(s)
                if j == last - 1 and step == 4:
                    for s in range(seqs // 2):
                        ctok(s).wait_recv()
                    for k in range(last - 1):
                        partner(0, PAIR, k)
                if j == last and step == 3:
                    if last < 2:
                        for s in range(seqs // 2):
                            tokens_in(s)
                            ctok(s).wait_recv()
                    for s in range(seqs // 2, seqs - 1):
                        tokens_in(s)
                    partner(0, PAIR, last - 1)
                    for s in range(seqs // 2, seqs - 1):
                        ctok(s).wait_recv()
                        for k in range(last):
                            partner(s, 1, k)
                if j == last and step == 4:
                    tokens_in(seqs - 1)
                    for s in range(seqs // 2):
                        for k in range(last - 1):
                            reduce(s, k)
                if j == last and step == 5:
                    ctok(seqs - 1).wait_recv()
                    for k in range(last):
                        partner(seqs - 1, 1, k)

        @pl.loop(4, n_a)
        def _(d):
            for bb in range(2):
                zstep(j, d, bb)

    if last == 0:
        weigh()
        for s in range(seqs):
            tokens_in(s)
        for s in range(seqs):
            ctok(s).wait_recv()
    yw_wait(False, last)
    accumulate(a, True)
    take(1)
    for s in range(seqs // 2):
        for k in range(max(last - 1, 0), last):
            reduce(s, k)
    for s in range(seqs // 2, seqs - 1):
        for k in range(last):
            reduce(s, k)
    take(2)
    for s in range(seqs // 2):
        for k in range(last - 1):
            collect(s, k)
    take(3)

    @pl.loop(4, n_a)
    def _(d):
        take(d)

    sums = [contract(acc[0], b, 0, seqs, last), contract(acc[1], ob, 0, seqs, last)]
    for s in range(seqs):
        part[s, last] = (sums[0][s] + sums[1][s]).astype(jnp.bfloat16)
    for s in range(seqs):
        rs_start(s, last)
    for k in range(last):
        reduce(seqs - 1, k)
    for s in range(seqs // 2):
        for k in range(max(last - 1, 0), last):
            collect(s, k)
    for s in range(seqs // 2, seqs - 1):
        for k in range(last):
            collect(s, k)
    for s in range(seqs):
        reduce(s, last)
    for j in range(last):
        for s in range(PAIR):
            yg(s, j, ob).wait_recv()
        finish(b, 0, j)
        finish(ob, 0, j)
    for j in range(last):
        for p in range(1, seqs // PAIR):
            for s in range(p * PAIR, (p + 1) * PAIR):
                if direct(s, j):
                    collect(s, j)
                yg(s, j, ob).wait_recv()
            finish(b, p, j)
            finish(ob, p, j)
        put(b, j).start()
        put(ob, j).start()
    normalize([side * n_c + j for side in range(2) for j in range(last)])
    for s in range(seqs):
        collect(s, last)
        yg(s, last, ob).wait_recv()
    for side in (b, ob):
        for p in range(seqs // PAIR):
            finish(side, p, last)
        put(side, last).start()
    normalize([side * n_c + last for side in range(2)])
    read_out = pltpu.make_async_copy(read_at, read, l_sem.at[0])
    read_out.start()

    for parity in range(2):
        @pl.when(a != reducer(parity))
        def _():
            drain(part.at[pl.ds(0, seqs // 2)], rs_s.at[parity])

        @pl.when(a == reducer(parity))
        def _():
            drain(got.at[pl.ds(0, n_a - 1)], ag_s)
            drain(got.at[:, :, 0], ac_s.at[0])
            if parity == (seqs - 1) % 2 and last > 0:
                drain(got.at[:, 0, pl.ds(0, last)], ac_s.at[1])

    if last > 0:
        drain(full.at[0, pl.ds(0, seqs - 1), pl.ds(0, last)], yg_s)
    drain(toks.at[0, pl.ds(0, rows // 2)], tok_s)
    drain(toks.at[0, pl.ds(0, rows // 2)], core_s)
    drain(tots.at[pl.ds(0, n_a - 1)], tot_s)
    yld.wait_send()
    drain(w.at[:, pl.ds(0, depth)], yw_s)
    drain(w.at[:, pl.ds(0, 2 * (n_a - 1) * depth), lanes(0)], x_s)
    for k in range(n_a):
        @pl.when(a == k)
        def _():
            if k < n_a - 1:
                drain(w.at[:, pl.ds(0, 2 * (k + 1) * depth), lanes(0)], z_s.at[1])
            if k > 0:
                drain(w.at[:, pl.ds(0, 2 * (n_a - k) * depth), lanes(0)], z_s.at[0])

    drain(staged, out_sem)
    read_out.wait()


def prompt_states(token_rows, key_weight, value_weight, decays, cos, sin, step, seqs, span, heads, n_sp):
    rows, width = token_rows.shape
    depth, whole = key_weight.shape
    cols = whole // 2
    n_c = cols // 128
    last = n_c - 1
    n_a = n_sp // 2
    hs = heads * seqs
    state_rows = seqs * HEAD_DIM
    dma = pltpu.SemaphoreType.DMA
    bf16 = jnp.bfloat16
    hbm = pl.BlockSpec(memory_space=pl.ANY)
    vmem = pl.BlockSpec(memory_space=pltpu.VMEM)
    operands = (token_rows, key_weight, value_weight, decays, cos, sin, *step)
    return pl.pallas_call(
        functools.partial(kernel, (n_sp, seqs, span, heads)),
        out_shape=(
            pltpu.VMEM((whole, state_rows), F32),
            pltpu.VMEM((seqs, whole), bf16),
        ),
        in_specs=[hbm] * 6 + [vmem] * 5,
        out_specs=(hbm, hbm),
        scratch_shapes=[
            pltpu.VMEM((whole, state_rows), F32),
            pltpu.VMEM((seqs, whole), bf16),
            pltpu.VMEM((2, rows, width), bf16),
            pltpu.VMEM((n_c, n_sp * depth, 256), bf16),
            pltpu.VMEM((2, hs, span), F32),
            pltpu.VMEM((n_a, 8, 128), F32),
            pltpu.VMEM((2, seqs, span, cols), F32),
            pltpu.VMEM((seqs, n_c, HEAD_DIM, 128), F32),
            pltpu.VMEM((seqs, n_c, HEAD_DIM, 128), bf16),
            pltpu.VMEM((n_a, seqs // 2, n_c, HEAD_DIM, 128), bf16),
            pltpu.VMEM((2, seqs, n_c, HEAD_DIM, 128), bf16),
            pltpu.VMEM((2 * span, 128), F32),
            pltpu.VMEM((2 * span, 128), F32),
            pltpu.VMEM((2, 8, 128), F32),
            pltpu.VMEM((state_rows, whole), F32),
            pltpu.VMEM((state_rows, whole), F32),
            pltpu.VMEM((seqs, whole), F32),
            pltpu.VMEM((2 * n_c, 8, 128), F32),
            pltpu.VMEM((2, rows, 256), F32),
            dma((6,)), dma((n_c,)), dma, dma((2, n_c)),
            dma, dma((seqs,)), dma, dma((seqs,)),
            dma((2,)), dma((n_c, n_sp)), dma, dma((last + n_a,)),
            dma, dma, dma, dma((n_a,)),
            dma((2,)), dma((seqs // 2, n_c)), dma, dma((seqs, n_c)),
            dma, dma((seqs, n_c)), dma((2,)), dma,
        ],
        compiler_params=pltpu.CompilerParams(
            collective_id=0, has_side_effects=True, vmem_limit_bytes=40 * 1024 * 1024
        ),
    )(*[pltpu.with_memory_space_constraint(v, pltpu.HBM) for v in operands])


def position_tables(length):
    half = HEAD_DIM // 2
    inverse = np.float32(10000.0) ** (-np.arange(half, dtype=np.float32) * np.float32(2.0 / HEAD_DIM))
    angles = np.arange(length + 8, dtype=np.float32)[:, None] * inverse[None, :].astype(np.float32)
    cosine = np.cos(angles.astype(np.float64)) * HEAD_DIM ** -0.5
    sine = np.sin(angles.astype(np.float64)) * HEAD_DIM ** -0.5
    cos = np.concatenate([cosine] * 4, axis=-1).astype(np.float32)
    sin = np.concatenate([-sine, sine] * 2, axis=-1).astype(np.float32)
    return cos, sin


def shards(
    tokens, key_weight, value_weight, log_decay, new_query, new_key, new_value, step_decay, norm_gain
):
    seqs, span, width = tokens.shape
    heads = key_weight.shape[1] // HEAD_DIM
    n_sp = lax.axis_size("sp")
    token_rows = tokens.reshape(seqs * span, width)
    decays = log_decay.reshape(heads * seqs, span)
    cos, sin = position_tables(span * n_sp)
    step = (new_query, new_key, new_value, step_decay.T, norm_gain.reshape(1, -1))
    state, read = prompt_states(
        token_rows, key_weight, value_weight, decays, jnp.asarray(cos), jnp.asarray(sin), step,
        seqs, span, heads, n_sp,
    )
    return (state.T.reshape(seqs * HEAD_DIM, heads, HEAD_DIM), read)


def solution(mesh):
    placed = (
        P("gr", "sp", None),
        P("sp", "tp"),
        P("sp", "tp"),
        P("tp", "gr", "sp"),
        P("gr", "tp"),
        P("gr", "tp"),
        P("gr", "tp"),
        P("tp", "gr"),
        P("tp"),
    )
    return jax.shard_map(
        shards,
        mesh=mesh,
        in_specs=placed,
        out_specs=(P("gr", "tp", None), P("gr", "tp")),
        check_vma=False,
    )
```

time: 161 us -> 97.1 us (0.60)
  Pallas kernels: 159 us -> 94.7 us
    pallas_call x1, Pallas kernels: 159 us -> 94.7 us  [prompt_states(): pl.pallas_call(functools.partial(kernel, (n_sp, seqs, span, heads)), out_...]
where the time goes in v2:
time: 97.1 us; the launch traced here: 96.9 us
  Pallas kernels  94.7 us (98%)
  local copies, waits for them, and re-layouts  1.57 us (2%)
    pallas_call x1, Pallas kernels, prompt_states(): pl.pallas_call(functools.partial(kernel, (n_sp, seqs, span, heads)), out_...  94.7 us

profile of v2, /device:TPU:0, one launch (start us, length us, event | category | flops | bytes accessed | tf_op | source)
XLA Modules:
  0.0 96.9 jit_solution(1785176280439461382)
XLA Ops:
  0.6 94.7 %shard_map.122 = (f32[1024,256]{1,0:T(8,128)S(1)}, bf16[4,1024]{1,0:T(4,128)(2,1)S(1)}) custom-call(bf16[512,4096]{1,0:T(8,128)(2,1)} %bitcast.8, bf16[512,1024]{1,0:T(8,128)(2,1)} %kw.1, bf16[512,1024]{1,0:T(8,128)(2,1)} %vw.1, f32[64,128]{1,0:T(8,128)} %bitcast.9, f32[1032,128]{1,0:T(8,128)} %constant.4.clone.cos_tab, f32[1032,128]{1,0:T(8,128)} %constant.5.clone.sin_tab, ...), custom_call_target="tpu_custom_call" | custom-call | tf_op jit(solution)/shard_map/pallas_call | solution.py:584
  95.3 1.0 %copy.15 = f32[256,16,64]{0,2,1:T(8,128)} copy(f32[256,16,64]{0,2,1:T(8,128)S(1)} %bitcast.7) | data formatting | bytes 2097152
  96.3 0.6 copy.16

commit v3 on v2

--- a/solution.py
+++ b/solution.py
@@ -17,11 +17,11 @@
 
 def kernel(
     sizes,
-    tok, kw, vw, ld, cos_tab, sin_tab, nq, nk, nv, sd, gain,
+    tok, kw, vw, ld, cos_tab, sin_tab, nq_in, nk_in, nv_in, sd_in, gain_in,
     out, read,
-    staged, read_at, toks, w, lds, tots, wts, own_state, part, got, full, cos_ref, sin_ref, ends, qx, outer, decay, raw_ref, acc,
+    nq, nk, nv, sd, gain, staged, read_at, toks, w, lds, tots, wts, own_state, part, got, full, cos_ref, sin_ref, ends, qx, outer, decay, raw_ref, acc,
     l_sem, w_sem, yw_s, yw_r, tok_s, tok_r, core_s, core_r, z_s, z_r, x_s, x_r,
-    ld_s, ld_r, tot_s, tot_r, rs_s, rs_r, ag_s, ag_r, yg_s, yg_r, ac_s, out_sem,
+    ld_s, ld_r, tot_s, tot_r, z_h, rs_s, rs_r, ag_s, ag_r, yg_s, yg_r, ac_s, out_sem,
 ):
     n_sp, seqs, span, heads = sizes
     n_a = n_sp // 2
@@ -45,6 +45,14 @@
     edge = jnp.logical_or(a == 0, a == n_a - 1)
     ahead = jnp.where(a < n_a // 2, 1, -1)
 
+    barrier = pltpu.get_barrier_semaphore()
+
+    @pl.loop(1, n_sp)
+    def _(k):
+        pl.semaphore_signal(barrier, inc=1, device_id=(g, lax.rem(sp + k, n_sp), tp), device_id_type=MESH)
+
+    pl.semaphore_signal(barrier, inc=1, device_id=x_peer, device_id_type=MESH)
+    pl.semaphore_signal(barrier, inc=1, device_id=core_peer, device_id_type=MESH)
     def lanes(m):
         return pl.ds(m * 128 if isinstance(m, int) else pl.multiple_of(m * 128, 128), 128)
 
@@ -66,6 +74,11 @@
         pltpu.make_async_copy(sin_tab.at[pl.ds(pl.multiple_of(a * 2 * span, 8), 2 * span)], sin_ref, l_sem.at[3]),
         pltpu.make_async_copy(cos_tab.at[pl.ds(n_sp * span, 8)], ends.at[0], l_sem.at[4]),
         pltpu.make_async_copy(sin_tab.at[pl.ds(n_sp * span, 8)], ends.at[1], l_sem.at[5]),
+        pltpu.make_async_copy(nq_in, nq, l_sem.at[6]),
+        pltpu.make_async_copy(nk_in, nk, l_sem.at[7]),
+        pltpu.make_async_copy(nv_in, nv, l_sem.at[8]),
+        pltpu.make_async_copy(sd_in, sd, l_sem.at[9]),
+        pltpu.make_async_copy(gain_in, gain, l_sem.at[10]),
     ]
     for j in range(n_c):
         for m in range(2):
@@ -73,14 +86,6 @@
     for c in local:
         c.start()
 
-    barrier = pltpu.get_barrier_semaphore()
-
-    @pl.loop(1, n_sp)
-    def _(k):
-        pl.semaphore_signal(barrier, inc=1, device_id=(g, lax.rem(sp + k, n_sp), tp), device_id_type=MESH)
-
-    pl.semaphore_signal(barrier, inc=1, device_id=x_peer, device_id_type=MESH)
-    pl.semaphore_signal(barrier, inc=1, device_id=core_peer, device_id_type=MESH)
     pl.semaphore_wait(barrier, n_sp + 1)
 
     def remote(src, dst, s, r, dev):
@@ -142,32 +147,41 @@
             def _():
                 yw(m, j).wait_recv()
 
-    def zsend(j, s, t):
-        ref = w.at[j, shard_rows(s), lanes(g)]
-        return remote(ref, ref, z_s.at[(t + 1) // 2], z_r.at[j, s], (g, sp + 2 * t, tp))
-
-    def xsend(j, s):
-        ref = w.at[j, shard_rows(s), lanes(g)]
+    def pieces(j, bb):
+        return 2 if (j, bb) in ((0, 0), (last, 1)) else 1
+
+    def piece(j, s, bb, q):
+        size = depth // pieces(j, bb)
+        return w.at[j, pl.ds(pl.multiple_of(s * depth + q * size, size), size), lanes(g)]
+
+    def zsend(j, s, bb, q, t):
+        ref = piece(j, s, bb, q)
+        arrived = z_r.at[j, s] if q == 0 else z_h.at[bb, s // 2]
+        return remote(ref, ref, z_s.at[(t + 1) // 2], arrived, (g, sp + 2 * t, tp))
+
+    def xsend(j, s, bb, q):
+        ref = piece(j, s, bb, q)
         return remote(ref, ref, x_s, x_r.at[j if j < last else last + s // 2], x_peer)
 
     def exists(place):
         return jnp.logical_and(place >= 0, place < n_a)
 
-    def launch(j, s):
+    def launch(j, s, bb):
         for t in (-ahead, ahead):
             @pl.when(exists(a + t))
             def _():
-                zsend(j, s, t).start()
+                for q in range(pieces(j, bb)):
+                    zsend(j, s, bb, q, t).start()
 
     def start_own(j):
         drain(w.at[j, shard_rows(sp)], w_sem.at[j])
-        launch(j, sp)
+        launch(j, sp, 0)
 
     def start_chunk(j):
         if j >= early:
             start_own(j)
         yw_wait(True, j)
-        launch(j, peer)
+        launch(j, peer, 1)
 
     def zstep(j, d, bb):
         side = b if bb == 0 else ob
@@ -175,13 +189,14 @@
             @pl.when(exists(a + t * d))
             def _():
                 s = (a + t * d) * 2 + side
-                zsend(j, s, -t).wait_recv()
-
-                @pl.when(exists(a - t))
-                def _():
-                    zsend(j, s, -t).start()
-
-                xsend(j, s).start()
+                for q in range(pieces(j, bb)):
+                    zsend(j, s, bb, q, -t).wait_recv()
+
+                    @pl.when(exists(a - t))
+                    def _():
+                        zsend(j, s, bb, q, -t).start()
+
+                    xsend(j, s, bb, q).start()
 
     def gather_x(j):
         yw_wait(False, j)
@@ -189,14 +204,13 @@
 
     for j in range(early):
         start_own(j)
-    start_chunk(0)
-
     def tsend(k):
         return remote(tots.at[a], tots.at[a], tot_s, tot_r.at[k], (g, lax.rem(a + k, n_a) * 2 + b, tp))
 
     for c in local:
         c.wait()
     raw_ref[...] = jnp.zeros(raw_ref.shape, F32)
+    acc[...] = jnp.zeros(acc.shape, F32)
     tots[a] = jnp.zeros(tots.shape[1:], F32)
 
     def shard_total(tb):
@@ -294,21 +308,29 @@
             result.append(jnp.where(lane_out < HEAD_DIM, term[:HEAD_DIM], term[HEAD_DIM:]))
         return result
 
-    def accumulate(place, fresh=False):
+    late_rows = rows - span
+    early_blocks = [(0, r, pair_rows) for r in range(0, rows, pair_rows)]
+    early_blocks += [(1, r, min(pair_rows, late_rows - r)) for r in range(0, late_rows, pair_rows)]
+    late_blocks = [(1, late_rows, span)]
+    all_blocks = [(k, r, pair_rows) for k in range(2) for r in range(0, rows, pair_rows)]
+
+    def accumulate(place, blocks):
         rows_at = pl.ds(pl.multiple_of(place * 2 * depth, 2 * depth), 2 * depth)
-        for k, tb in enumerate((b, ob)):
-            for r in range(0, rows, pair_rows):
-                new = jnp.dot(
-                    toks[tb, r:r + pair_rows, rows_at], w[last, rows_at, :], preferred_element_type=F32
-                )
-                acc[k, r:r + pair_rows] = new if fresh else acc[k, r:r + pair_rows] + new
-
-    def take(d):
-        for t in (ahead, -ahead):
-            @pl.when(exists(a + t * d))
-            def _():
-                drain(w.at[last, pl.ds(0, 2 * depth), lanes(0)], x_r.at[last + a + t * d])
-                accumulate(a + t * d)
+        for k, r, n in blocks:
+            acc[k, r:r + n] += jnp.dot(
+                toks[ob if k else b, r:r + n, rows_at], w[last, rows_at, :], preferred_element_type=F32
+            )
+
+    behind = jnp.where(ahead > 0, a, n_a - 1 - a)
+
+    def place(i):
+        paired = i < 2 * behind
+        step = jnp.where(paired, i // 2 + 1, i - behind + 1)
+        return a + jnp.where(jnp.logical_and(paired, i % 2 == 1), -ahead, ahead) * step
+
+    def take(i, blocks):
+        drain(w.at[last, pl.ds(0, 2 * depth), lanes(0)], x_r.at[last + place(i)])
+        accumulate(place(i), blocks)
 
     def own(j):
         @pl.loop(0, seqs // PAIR)
@@ -316,21 +338,24 @@
             for i, state in enumerate(states(b, p * PAIR, PAIR, j)):
                 own_state[p * PAIR + i, j] = state
 
-    def reducer(s):
-        return n_a // 2 - 1 + s % 2
+    def reducer(s, j):
+        return n_a // 2 - 1 + (s + j) % 2
 
     def rs(s, j):
-        to = reducer(s)
-        return remote(part.at[s, j], got.at[a, s // 2, j], rs_s.at[s % 2], rs_r.at[s // 2, j], (g, to * 2 + b, tp))
-
-    def partner(s, n, j):
-        for i, state in enumerate(states(ob, s, n, j)):
-            part[s + i, j] = (own_state[s + i, j] + state).astype(jnp.bfloat16)
-        for i in range(n):
-            rs_start(s + i, j)
+        to = reducer(s, j)
+        return remote(part.at[s, j], got.at[a, s // 2, j], rs_s.at[(s + j) % 2], rs_r.at[s // 2, j], (g, to * 2 + b, tp))
+
+    def partner(s, n, chunks):
+        ready = [states(ob, s, n, j) for j in chunks]
+        for j, of_chunk in zip(chunks, ready):
+            for i in range(n):
+                part[s + i, j] = (own_state[s + i, j] + of_chunk[i]).astype(jnp.bfloat16)
+        for j in chunks:
+            for i in range(n):
+                rs_start(s + i, j)
 
     def rs_start(s, j):
-        @pl.when(a != reducer(s))
+        @pl.when(a != reducer(s, j))
         def _():
             rs(s, j).start()
 
@@ -338,19 +363,19 @@
         here = full.at[b, s, j]
         return remote(here, here, ag_s, ag_r.at[s, j], (g, to * 2 + b, tp))
 
-    def direct(s, j):
-        return s == seqs - 1 or j == last
+    def direct(j):
+        return j == last
 
     def across(s, j, to):
         here = full.at[b, s, j]
-        return remote(here, here, ac_s.at[0 if j == last else 1], yg_r.at[s, j], (g, to * 2 + ob, tp))
+        return remote(here, here, ac_s, yg_r.at[s, j], (g, to * 2 + ob, tp))
 
     def yg(s, j, side):
         here = full.at[side, s, j]
         return remote(here, here, yg_s, yg_r.at[s, j], y_peer)
 
     def reduce(s, j):
-        @pl.when(a == reducer(s))
+        @pl.when(a == reducer(s, j))
         def _():
             drain(got.at[pl.ds(0, n_a - 1), s // 2, j], rs_r.at[s // 2, j])
 
@@ -363,20 +388,20 @@
             @pl.loop(1, n_a)
             def _(k):
                 to = lax.rem(a + k, n_a)
-                if direct(s, j):
+                if direct(j):
                     across(s, j, to).start()
                 ag(s, j, to).start()
 
-            if direct(s, j):
+            if direct(j):
                 across(s, j, a).start()
             else:
                 yg(s, j, b).start()
 
     def collect(s, j):
-        @pl.when(a != reducer(s))
+        @pl.when(a != reducer(s, j))
         def _():
             ag(s, j, a).wait_recv()
-            if not direct(s, j):
+            if not direct(j):
                 yg(s, j, b).start()
 
     def finish(side, p, j):
@@ -416,8 +441,19 @@
             def _():
                 start_chunk(j)
 
+        turns = [[(j, step // 2 + 1, step % 2)] for step in range(6)]
+        if early > 1 and j == 0:
+            turns = [
+                [(0, 1, 0)], [(1, 1, 0), (0, 2, 0)], [(0, 1, 1), (1, 2, 0)],
+                [(0, 3, 0)], [(0, 2, 1), (1, 3, 0)], [(0, 3, 1)],
+            ]
+        if early > 1 and j == 1:
+            turns = [[], [(1, 1, 1)], [(1, 2, 1)], [(1, 3, 1)], [], []]
         for step in range(6):
-            zstep(j, step // 2 + 1, step % 2)
+            for turn in turns[step]:
+                zstep(*turn)
+            if j == 0 and step == 0:
+                start_chunk(0)
             if step == 2 and j < last:
                 @pl.when(edge)
                 def _():
@@ -430,6 +466,9 @@
             else:
                 if j == 1 and step == 1:
                     weigh()
+                if j == last and step == 1:
+                    for s in range(0 if last < 2 else seqs // 2, seqs - 1):
+                        tokens_in(s)
                 if step == 2:
                     gather_x(j - 1)
                     own(j - 1)
@@ -439,29 +478,20 @@
                 if j == last - 1 and step == 4:
                     for s in range(seqs // 2):
                         ctok(s).wait_recv()
-                    for k in range(last - 1):
-                        partner(0, PAIR, k)
+                    partner(0, PAIR, range(last - 1))
                 if j == last and step == 3:
-                    if last < 2:
-                        for s in range(seqs // 2):
-                            tokens_in(s)
-                            ctok(s).wait_recv()
+                    for s in range(0 if last < 2 else seqs // 2, seqs - 1):
+                        ctok(s).wait_recv()
+                    partner(0, PAIR, [last - 1])
                     for s in range(seqs // 2, seqs - 1):
-                        tokens_in(s)
-                    partner(0, PAIR, last - 1)
+                        partner(s, 1, [0])
+                if j == last and step == 4:
                     for s in range(seqs // 2, seqs - 1):
-                        ctok(s).wait_recv()
-                        for k in range(last):
-                            partner(s, 1, k)
-                if j == last and step == 4:
-                    tokens_in(seqs - 1)
+                        partner(s, 1, range(1, last))
                     for s in range(seqs // 2):
                         for k in range(last - 1):
                             reduce(s, k)
-                if j == last and step == 5:
-                    ctok(seqs - 1).wait_recv()
-                    for k in range(last):
-                        partner(seqs - 1, 1, k)
+                    tokens_in(seqs - 1)
 
         @pl.loop(4, n_a)
         def _(d):
@@ -474,24 +504,26 @@
             tokens_in(s)
         for s in range(seqs):
             ctok(s).wait_recv()
+    take(0, early_blocks)
+    take(1, early_blocks)
     yw_wait(False, last)
-    accumulate(a, True)
-    take(1)
-    for s in range(seqs // 2):
-        for k in range(max(last - 1, 0), last):
+    accumulate(a, early_blocks)
+    if last > 0:
+        ctok(seqs - 1).wait_recv()
+    partner(seqs - 1, 1, range(last))
+    for s in range(seqs - 1):
+        for k in range(last - 1 if s < seqs // 2 else 0, last):
             reduce(s, k)
-    for s in range(seqs // 2, seqs - 1):
-        for k in range(last):
-            reduce(s, k)
-    take(2)
     for s in range(seqs // 2):
         for k in range(last - 1):
             collect(s, k)
-    take(3)
-
-    @pl.loop(4, n_a)
-    def _(d):
-        take(d)
+    accumulate(a, late_blocks)
+    accumulate(place(0), late_blocks)
+    accumulate(place(1), late_blocks)
+
+    @pl.loop(2, n_a - 1)
+    def _(i):
+        take(i, all_blocks)
 
     sums = [contract(acc[0], b, 0, seqs, last), contract(acc[1], ob, 0, seqs, last)]
     for s in range(seqs):
@@ -500,14 +532,14 @@
         rs_start(s, last)
     for k in range(last):
         reduce(seqs - 1, k)
+    for s in range(seqs):
+        reduce(s, last)
     for s in range(seqs // 2):
         for k in range(max(last - 1, 0), last):
             collect(s, k)
-    for s in range(seqs // 2, seqs - 1):
+    for s in range(seqs // 2, seqs):
         for k in range(last):
             collect(s, k)
-    for s in range(seqs):
-        reduce(s, last)
     for j in range(last):
         for s in range(PAIR):
             yg(s, j, ob).wait_recv()
@@ -516,8 +548,6 @@
     for j in range(last):
         for p in range(1, seqs // PAIR):
             for s in range(p * PAIR, (p + 1) * PAIR):
-                if direct(s, j):
-                    collect(s, j)
                 yg(s, j, ob).wait_recv()
             finish(b, p, j)
             finish(ob, p, j)
@@ -536,19 +566,17 @@
     read_out.start()
 
     for parity in range(2):
-        @pl.when(a != reducer(parity))
+        @pl.when(a != reducer(parity, 0))
         def _():
             drain(part.at[pl.ds(0, seqs // 2)], rs_s.at[parity])
 
-        @pl.when(a == reducer(parity))
+        @pl.when(a == reducer(parity, 0))
         def _():
             drain(got.at[pl.ds(0, n_a - 1)], ag_s)
-            drain(got.at[:, :, 0], ac_s.at[0])
-            if parity == (seqs - 1) % 2 and last > 0:
-                drain(got.at[:, 0, pl.ds(0, last)], ac_s.at[1])
+            drain(got.at[:, :, 0], ac_s)
 
     if last > 0:
-        drain(full.at[0, pl.ds(0, seqs - 1), pl.ds(0, last)], yg_s)
+        drain(full.at[0, :, pl.ds(0, last)], yg_s)
     drain(toks.at[0, pl.ds(0, rows // 2)], tok_s)
     drain(toks.at[0, pl.ds(0, rows // 2)], core_s)
     drain(tots.at[pl.ds(0, n_a - 1)], tot_s)
@@ -567,6 +595,14 @@
     read_out.wait()
 
 
+def store(state, read, out, read_out, sem):
+    copies = [pltpu.make_async_copy(state, out, sem.at[0]), pltpu.make_async_copy(read, read_out, sem.at[1])]
+    for c in copies:
+        c.start()
+    for c in copies:
+        c.wait()
+
+
 def prompt_states(token_rows, key_weight, value_weight, decays, cos, sin, step, seqs, span, heads, n_sp):
     rows, width = token_rows.shape
     depth, whole = key_weight.shape
@@ -579,17 +615,17 @@
     dma = pltpu.SemaphoreType.DMA
     bf16 = jnp.bfloat16
     hbm = pl.BlockSpec(memory_space=pl.ANY)
-    vmem = pl.BlockSpec(memory_space=pltpu.VMEM)
     operands = (token_rows, key_weight, value_weight, decays, cos, sin, *step)
-    return pl.pallas_call(
+    state, read = pl.pallas_call(
         functools.partial(kernel, (n_sp, seqs, span, heads)),
         out_shape=(
             pltpu.VMEM((whole, state_rows), F32),
             pltpu.VMEM((seqs, whole), bf16),
         ),
-        in_specs=[hbm] * 6 + [vmem] * 5,
+        in_specs=[hbm] * 11,
         out_specs=(hbm, hbm),
         scratch_shapes=[
+            *(pltpu.VMEM(v.shape, v.dtype) for v in step),
             pltpu.VMEM((whole, state_rows), F32),
             pltpu.VMEM((seqs, whole), bf16),
             pltpu.VMEM((2, rows, width), bf16),
@@ -609,17 +645,25 @@
             pltpu.VMEM((seqs, whole), F32),
             pltpu.VMEM((2 * n_c, 8, 128), F32),
             pltpu.VMEM((2, rows, 256), F32),
-            dma((6,)), dma((n_c,)), dma, dma((2, n_c)),
+            dma((11,)), dma((n_c,)), dma, dma((2, n_c)),
             dma, dma((seqs,)), dma, dma((seqs,)),
             dma((2,)), dma((n_c, n_sp)), dma, dma((last + n_a,)),
-            dma, dma, dma, dma((n_a,)),
+            dma, dma, dma, dma((n_a,)), dma((2, n_a)),
             dma((2,)), dma((seqs // 2, n_c)), dma, dma((seqs, n_c)),
-            dma, dma((seqs, n_c)), dma((2,)), dma,
+            dma, dma((seqs, n_c)), dma, dma,
         ],
         compiler_params=pltpu.CompilerParams(
             collective_id=0, has_side_effects=True, vmem_limit_bytes=40 * 1024 * 1024
         ),
     )(*[pltpu.with_memory_space_constraint(v, pltpu.HBM) for v in operands])
+    return pl.pallas_call(
+        store,
+        out_shape=(pltpu.HBM(state.shape, state.dtype), pltpu.HBM(read.shape, read.dtype)),
+        in_specs=[pl.BlockSpec(memory_space=pltpu.VMEM)] * 2,
+        out_specs=(hbm, hbm),
+        scratch_shapes=[dma((2,))],
+        compiler_params=pltpu.CompilerParams(vmem_limit_bytes=8 * 1024 * 1024),
+    )(*[pltpu.with_memory_space_constraint(v, pltpu.VMEM) for v in (state, read)])
 
 
 def position_tables(length):

time: 97.1 us -> 95.5 us (0.984)
  local copies, waits for them, and re-layouts: 1.57 us -> 0 us
    unnamed x2 -> x0, local copies, waits for them, and re-layouts: 1.57 us -> none
    pallas_call x1, Pallas kernels: 94.7 us -> 93.6 us  [prompt_states(): pl.pallas_call(functools.partial(kernel, (n_sp, seqs, span, heads)), out_...]
    pallas_call x0 -> x1, Pallas kernels: none -> 0.99 us  [prompt_states(): pl.pallas_call(store, out_shape=(pltpu.HBM(state.shape, state.dtype), plt...]
where the time goes in v3:
time: 95.5 us; the launch traced here: 95.4 us
  Pallas kernels  94.6 us (99%)
    pallas_call x1, Pallas kernels, prompt_states(): pl.pallas_call(functools.partial(kernel, (n_sp, seqs, span, heads)), out_...  93.6 us

profile of v3, /device:TPU:0, one launch (start us, length us, event | category | flops | bytes accessed | tf_op | source)
XLA Modules:
  0.0 95.4 jit_solution(11092311079910098628)
XLA Ops:
  0.6 93.6 %shard_map.122 = (f32[1024,256]{1,0:T(8,128)S(1)}, bf16[4,1024]{1,0:T(4,128)(2,1)S(1)}) custom-call(bf16[512,4096]{1,0:T(8,128)(2,1)} %bitcast.7, bf16[512,1024]{1,0:T(8,128)(2,1)} %kw.1, bf16[512,1024]{1,0:T(8,128)(2,1)} %vw.1, f32[64,128]{1,0:T(8,128)} %bitcast.8, f32[1032,128]{1,0:T(8,128)} %constant.4.clone.cos_tab, f32[1032,128]{1,0:T(8,128)} %constant.5.clone.sin_tab, ...), custom_call_target="tpu_custom_call" | custom-call | tf_op jit(solution)/shard_map/pallas_call | solution.py:619
  94.2 1.0 %shard_map.123 = (f32[1024,256]{1,0:T(8,128)}, bf16[4,1024]{1,0:T(4,128)(2,1)}) custom-call(f32[1024,256]{1,0:T(8,128)S(1)} %get-tuple-element.6.state, bf16[4,1024]{1,0:T(4,128)(2,1)S(1)} %get-tuple-element.7.read), custom_call_target="tpu_custom_call" | custom-call | tf_op jit(solution)/shard_map/pallas_call | solution.py:659

commit v4 on v3

--- a/solution.py
+++ b/solution.py
@@ -363,12 +363,12 @@
         here = full.at[b, s, j]
         return remote(here, here, ag_s, ag_r.at[s, j], (g, to * 2 + b, tp))
 
-    def direct(j):
-        return j == last
+    def direct(s, j):
+        return j == last or s == seqs - 1
 
     def across(s, j, to):
         here = full.at[b, s, j]
-        return remote(here, here, ac_s, yg_r.at[s, j], (g, to * 2 + ob, tp))
+        return remote(here, here, ac_s.at[0 if j == last else 1], yg_r.at[s, j], (g, to * 2 + ob, tp))
 
     def yg(s, j, side):
         here = full.at[side, s, j]
@@ -388,11 +388,11 @@
             @pl.loop(1, n_a)
             def _(k):
                 to = lax.rem(a + k, n_a)
-                if direct(j):
+                if direct(s, j):
                     across(s, j, to).start()
                 ag(s, j, to).start()
 
-            if direct(j):
+            if direct(s, j):
                 across(s, j, a).start()
             else:
                 yg(s, j, b).start()
@@ -401,7 +401,7 @@
         @pl.when(a != reducer(s, j))
         def _():
             ag(s, j, a).wait_recv()
-            if not direct(j):
+            if not direct(s, j):
                 yg(s, j, b).start()
 
     def finish(side, p, j):
@@ -508,12 +508,12 @@
     take(1, early_blocks)
     yw_wait(False, last)
     accumulate(a, early_blocks)
+    for s in range(seqs - 1):
+        for k in range(last - 1 if s < seqs // 2 else 0, last):
+            reduce(s, k)
     if last > 0:
         ctok(seqs - 1).wait_recv()
     partner(seqs - 1, 1, range(last))
-    for s in range(seqs - 1):
-        for k in range(last - 1 if s < seqs // 2 else 0, last):
-            reduce(s, k)
     for s in range(seqs // 2):
         for k in range(last - 1):
             collect(s, k)
@@ -530,16 +530,15 @@
         part[s, last] = (sums[0][s] + sums[1][s]).astype(jnp.bfloat16)
     for s in range(seqs):
         rs_start(s, last)
+    for s in range(seqs - 1):
+        for k in range(last - 1 if s < seqs // 2 else 0, last):
+            collect(s, k)
     for k in range(last):
         reduce(seqs - 1, k)
     for s in range(seqs):
         reduce(s, last)
-    for s in range(seqs // 2):
-        for k in range(max(last - 1, 0), last):
-            collect(s, k)
-    for s in range(seqs // 2, seqs):
-        for k in range(last):
-            collect(s, k)
+    for k in range(last):
+        collect(seqs - 1, k)
     for j in range(last):
         for s in range(PAIR):
             yg(s, j, ob).wait_recv()
@@ -573,10 +572,13 @@
         @pl.when(a == reducer(parity, 0))
         def _():
             drain(got.at[pl.ds(0, n_a - 1)], ag_s)
-            drain(got.at[:, :, 0], ac_s)
+            drain(got.at[:, :, 0], ac_s.at[0])
+            late = len([k for k in range(last) if (seqs - 1 + k) % 2 == parity])
+            if late:
+                drain(got.at[:, 0, pl.ds(0, late)], ac_s.at[1])
 
     if last > 0:
-        drain(full.at[0, :, pl.ds(0, last)], yg_s)
+        drain(full.at[0, pl.ds(0, seqs - 1), pl.ds(0, last)], yg_s)
     drain(toks.at[0, pl.ds(0, rows // 2)], tok_s)
     drain(toks.at[0, pl.ds(0, rows // 2)], core_s)
     drain(tots.at[pl.ds(0, n_a - 1)], tot_s)
@@ -650,7 +652,7 @@
             dma((2,)), dma((n_c, n_sp)), dma, dma((last + n_a,)),
             dma, dma, dma, dma((n_a,)), dma((2, n_a)),
             dma((2,)), dma((seqs // 2, n_c)), dma, dma((seqs, n_c)),
-            dma, dma((seqs, n_c)), dma, dma,
+            dma, dma((seqs, n_c)), dma((2,)), dma,
         ],
         compiler_params=pltpu.CompilerParams(
             collective_id=0, has_side_effects=True, vmem_limit_bytes=40 * 1024 * 1024

time: 95.5 us -> 95.3 us (level)
  no operation moved by 1% of the time
where the time goes in v4:
time: 95.3 us; the launch traced here: 95.2 us
  Pallas kernels  94.4 us (99%)
    pallas_call x1, Pallas kernels, prompt_states(): pl.pallas_call(functools.partial(kernel, (n_sp, seqs, span, heads)), out_...  93.4 us

profile of v4, /device:TPU:0, one launch (start us, length us, event | category | flops | bytes accessed | tf_op | source)
XLA Modules:
  0.0 95.2 jit_solution(10248341202653989374)
XLA Ops:
  0.6 93.4 %shard_map.122 = (f32[1024,256]{1,0:T(8,128)S(1)}, bf16[4,1024]{1,0:T(4,128)(2,1)S(1)}) custom-call(bf16[512,4096]{1,0:T(8,128)(2,1)} %bitcast.7, bf16[512,1024]{1,0:T(8,128)(2,1)} %kw.1, bf16[512,1024]{1,0:T(8,128)(2,1)} %vw.1, f32[64,128]{1,0:T(8,128)} %bitcast.8, f32[1032,128]{1,0:T(8,128)} %constant.4.clone.cos_tab, f32[1032,128]{1,0:T(8,128)} %constant.5.clone.sin_tab, ...), custom_call_target="tpu_custom_call" | custom-call | tf_op jit(solution)/shard_map/pallas_call | solution.py:621
  94.0 1.0 %shard_map.123 = (f32[1024,256]{1,0:T(8,128)}, bf16[4,1024]{1,0:T(4,128)(2,1)}) custom-call(f32[1024,256]{1,0:T(8,128)S(1)} %get-tuple-element.6.state, bf16[4,1024]{1,0:T(4,128)(2,1)S(1)} %get-tuple-element.7.read), custom_call_target="tpu_custom_call" | custom-call | tf_op jit(solution)/shard_map/pallas_call | solution.py:661

commit v5 on v4

--- a/solution.py
+++ b/solution.py
@@ -388,9 +388,9 @@
             @pl.loop(1, n_a)
             def _(k):
                 to = lax.rem(a + k, n_a)
+                ag(s, j, to).start()
                 if direct(s, j):
                     across(s, j, to).start()
-                ag(s, j, to).start()
 
             if direct(s, j):
                 across(s, j, a).start()
@@ -491,6 +491,7 @@
                     for s in range(seqs // 2):
                         for k in range(last - 1):
                             reduce(s, k)
+                    take(0, early_blocks)
                     tokens_in(seqs - 1)
 
         @pl.loop(4, n_a)
@@ -504,7 +505,8 @@
             tokens_in(s)
         for s in range(seqs):
             ctok(s).wait_recv()
-    take(0, early_blocks)
+    if last == 0:
+        take(0, early_blocks)
     take(1, early_blocks)
     yw_wait(False, last)
     accumulate(a, early_blocks)
@@ -555,11 +557,14 @@
     normalize([side * n_c + j for side in range(2) for j in range(last)])
     for s in range(seqs):
         collect(s, last)
+    for p in range(seqs // PAIR):
+        finish(b, p, last)
+    put(b, last).start()
+    for s in range(seqs):
         yg(s, last, ob).wait_recv()
-    for side in (b, ob):
-        for p in range(seqs // PAIR):
-            finish(side, p, last)
-        put(side, last).start()
+    for p in range(seqs // PAIR):
+        finish(ob, p, last)
+    put(ob, last).start()
     normalize([side * n_c + last for side in range(2)])
     read_out = pltpu.make_async_copy(read_at, read, l_sem.at[0])
     read_out.start()

time: 95.3 us -> 95.4 us (level)
  no operation moved by 1% of the time
where the time goes in v5:
time: 95.4 us; the launch traced here: 95.2 us
  Pallas kernels  94.4 us (99%)
    pallas_call x1, Pallas kernels, prompt_states(): pl.pallas_call(functools.partial(kernel, (n_sp, seqs, span, heads)), out_...  93.4 us

profile of v5, /device:TPU:0, one launch (start us, length us, event | category | flops | bytes accessed | tf_op | source)
XLA Modules:
  0.0 95.2 jit_solution(6814244265447321866)
XLA Ops:
  0.6 93.4 %shard_map.122 = (f32[1024,256]{1,0:T(8,128)S(1)}, bf16[4,1024]{1,0:T(4,128)(2,1)S(1)}) custom-call(bf16[512,4096]{1,0:T(8,128)(2,1)} %bitcast.7, bf16[512,1024]{1,0:T(8,128)(2,1)} %kw.1, bf16[512,1024]{1,0:T(8,128)(2,1)} %vw.1, f32[64,128]{1,0:T(8,128)} %bitcast.8, f32[1032,128]{1,0:T(8,128)} %constant.4.clone.cos_tab, f32[1032,128]{1,0:T(8,128)} %constant.5.clone.sin_tab, ...), custom_call_target="tpu_custom_call" | custom-call | tf_op jit(solution)/shard_map/pallas_call | solution.py:626
  94.1 1.0 %shard_map.123 = (f32[1024,256]{1,0:T(8,128)}, bf16[4,1024]{1,0:T(4,128)(2,1)}) custom-call(f32[1024,256]{1,0:T(8,128)S(1)} %get-tuple-element.6.state, bf16[4,1024]{1,0:T(4,128)(2,1)S(1)} %get-tuple-element.7.read), custom_call_target="tpu_custom_call" | custom-call | tf_op jit(solution)/shard_map/pallas_call | solution.py:666
